TPU v7x, 32 devices: a whole 2x2x4 slice. The times are simulated.
32 devices in a mesh: sp: 8 (over z, x), dp: 4 (over y, core).
Axes of the slice: x: 2, y: 2, z: 4, core: 2. Of those that a mesh axis runs over, the one named last changes fastest.
Arguments:
- queries: bfloat16 [4, 1024, 16, 128], P('dp', 'sp'), may hold values from -6 to 6
- key_rows: bfloat16 [4, 1024, 4, 128], P('dp', 'sp'), may hold values from -6 to 6
- values: bfloat16 [4, 1024, 4, 128], P('dp', 'sp'), may hold values from -6 to 6
- query_gain: float32 [128], replicated, may hold values from 0.4 to 5
- key_gain: float32 [128], replicated, may hold values from 0.4 to 5
- out_weight: bfloat16 [2048, 2048], P('sp', 'dp'), may hold values from -0.125 to 0.125
- residual: bfloat16 [4, 1024, 2048], P('dp', 'sp'), may hold values from -6 to 6
- norm_gain: float32 [2048], replicated, may hold values from 0.1 to 1.9
- expert_gate: bfloat16 [8, 2048, 1792], P('sp'), may hold values from -0.125 to 0.125
- expert_up: bfloat16 [8, 2048, 1792], P('sp'), may hold values from -0.125 to 0.125
- expert_down: bfloat16 [8, 1792, 2048], P('sp'), may hold values from -0.125 to 0.125
- routes: int32 [4, 1024, 2], P('dp', 'sp'), may hold values from 0 to 7, all different within a row; in each aligned block of 64 rows (0 to 63, 64 to 127, ..., all dimensions but the last counted through in order) at most 32 rows name the same one
- route_weight: float32 [4, 1024, 2], P('dp', 'sp'), may hold values from 0.25 to 1
Outputs:
- layer_out: bfloat16 [4, 1024, 2048], P('dp', 'sp')
Inputs may be any that keep to these rules, and one draw needn't show every extreme that they name: `routes`: in each aligned block of 64 rows of one device, no expert is named by more than 32 entries, a bound that some block reaches; the two experts of a row differ.
All inputs are finite; a program needn't handle non-finite values.
Results may differ from a plain program's by a relative error of at most 0.0095.
The roundings to bfloat16 on the way count: a program that leaves them out, or rounds other values in their place, can miss the bound.
Values may be sent and summed in bfloat16 or wider, within the bound.
No kernel may reach another device: no remote copies, remote signals or barrier semaphores. Data moves between devices by JAX's collectives and lax.ppermute only.
A program may use at most 128 MiB of HBM per device.

v0:
```python
import jax
import jax.numpy as jnp
from jax import lax
from jax.sharding import PartitionSpec as P

GRID_W = 64


EPS = 1e-06
THETA = 10000.0


def rotate_half(vector, position):
    half_size = vector.shape[-1] // 2
    inverse = THETA ** (-jnp.arange(half_size, dtype=jnp.float32) / half_size)
    angles = position[:, None] * inverse[None, :]
    cosine = jnp.cos(angles)[:, None, :]
    sine_part = jnp.sin(angles)[:, None, :]
    first_part = vector[..., :half_size]
    second_part = vector[..., half_size:]
    return jnp.concatenate(
        [
            first_part * cosine - second_part * sine_part,
            first_part * sine_part + second_part * cosine,
        ],
        axis=-1,
    )


def normalize_rotate(vector, gain, positions):
    as_float = vector.astype(jnp.float32)
    scaled = (
        as_float * lax.rsqrt(jnp.mean(as_float * as_float, axis=-1, keepdims=True) + EPS) * gain
    )
    grid_row = (positions // GRID_W).astype(jnp.float32)
    column = (positions % GRID_W).astype(jnp.float32)
    quarter = scaled.shape[-1] // 2
    turned = jnp.concatenate(
        [rotate_half(scaled[..., :quarter], grid_row), rotate_half(scaled[..., quarter:], column)],
        axis=-1,
    )
    return turned.astype(jnp.bfloat16)


def softmax_rows(scores):
    row_max = jnp.max(scores, axis=-1, keepdims=True)
    exponent = jnp.exp(scores - row_max)
    return (exponent / jnp.sum(exponent, axis=-1, keepdims=True)).astype(jnp.bfloat16)


def attend_block(query_rows, key_rows, value_rows):
    scores = jnp.einsum(
        "qd,kd->qk", query_rows, key_rows, preferred_element_type=jnp.float32
    ) * query_rows.shape[-1] ** (-0.5)
    weights = softmax_rows(scores)
    return jnp.dot(weights, value_rows, preferred_element_type=jnp.float32).astype(jnp.bfloat16)


def attend_heads(head_query, head_key, head_value):
    length, head_count, head_width = head_query.shape
    block_size = min(512, length)
    outputs = []
    for head_index in range(head_count):
        key_slice = head_key[:, head_index]
        value_slice = head_value[:, head_index]
        query_blocks = head_query[:, head_index].reshape(
            length // block_size, block_size, head_width
        )

        def one_block(query_block):
            return attend_block(query_block, key_slice, value_slice)

        outputs.append(lax.map(one_block, query_blocks).reshape(length, head_width))
    return jnp.stack(outputs, axis=1)


def project_tokens(attended, out_weight):
    all_rows = lax.all_gather(attended[None], "dp", axis=0, tiled=True)
    local_cols = lax.all_gather(out_weight, "sp", axis=0, tiled=True)
    partial_cols = jnp.einsum(
        "std,dc->stc", all_rows, local_cols, preferred_element_type=jnp.float32
    )
    back_cols = lax.all_to_all(
        partial_cols.astype(jnp.bfloat16), "dp", split_axis=0, concat_axis=2, tiled=True
    ).astype(partial_cols.dtype)
    return back_cols[0]


def on_device(
    queries,
    key_rows,
    values,
    query_gain,
    key_gain,
    out_weight,
    residual,
    norm_gain,
    expert_gate,
    expert_up,
    expert_down,
    routes,
    route_weight,
):
    tok_count = queries.shape[1]
    head_count = queries.shape[2]
    head_width = queries.shape[3]
    group_size = head_count // key_rows.shape[2]
    positions = lax.axis_index("sp") * tok_count + jnp.arange(tok_count, dtype=jnp.int32)
    rot_query = normalize_rotate(queries[0], query_gain, positions)
    rot_key = normalize_rotate(key_rows[0], key_gain, positions)
    value_rows = values[0]
    head_query, head_key, head_value = (
        lax.all_to_all(rot_query, "sp", split_axis=1, concat_axis=0, tiled=True),
        lax.all_to_all(
            jnp.repeat(rot_key, group_size, axis=1), "sp", split_axis=1, concat_axis=0, tiled=True
        ),
        lax.all_to_all(
            jnp.repeat(value_rows, group_size, axis=1),
            "sp",
            split_axis=1,
            concat_axis=0,
            tiled=True,
        ),
    )
    by_heads = attend_heads(head_query, head_key, head_value)
    returned_heads = lax.all_to_all(by_heads, "sp", split_axis=0, concat_axis=1, tiled=True)
    projected = project_tokens(
        returned_heads.reshape(tok_count, head_count * head_width), out_weight
    )
    mixed_sum = residual[0].astype(jnp.float32) + projected
    normed = (
        mixed_sum
        * lax.rsqrt(jnp.mean(mixed_sum * mixed_sum, axis=-1, keepdims=True) + EPS)
        * norm_gain
    ).astype(jnp.bfloat16)
    experts = expert_gate.shape[0] * lax.axis_size("sp")
    half_rows = tok_count // 2
    capacity = max(2, 4 * half_rows // experts)
    chosen = routes[0].reshape(2, half_rows * 2)
    onehot = (chosen[..., None] == jnp.arange(experts, dtype=jnp.int32)).astype(jnp.int32)
    slot_rank = jnp.sum(jnp.cumsum(onehot, axis=1) * onehot, axis=-1) - 1
    slot_index = jnp.arange(2, dtype=jnp.int32)[:, None] * capacity + slot_rank
    target = (chosen * (2 * capacity) + slot_index).reshape(-1)
    model_width = normed.shape[1]
    filled = (
        jnp.zeros((experts * 2 * capacity, model_width), jnp.bfloat16)
        .at[target]
        .set(jnp.repeat(normed, 2, axis=0))
    )
    buffer = filled.reshape(experts, 2 * capacity, model_width)
    slot_batch = lax.all_to_all(buffer, "sp", split_axis=0, concat_axis=0, tiled=True)
    sources, slot_count, feature_count = slot_batch.shape
    flat_rows = slot_batch.reshape(sources * slot_count, feature_count)
    gate_part = jnp.dot(flat_rows, expert_gate[0], preferred_element_type=jnp.float32)
    up_part = jnp.dot(flat_rows, expert_up[0], preferred_element_type=jnp.float32)
    hidden = (jax.nn.silu(gate_part) * up_part).astype(jnp.bfloat16)
    expert_result = jnp.dot(hidden, expert_down[0], preferred_element_type=jnp.float32).astype(
        jnp.bfloat16
    )
    served = expert_result.reshape(sources, slot_count, feature_count)
    returned = lax.all_to_all(served, "sp", split_axis=0, concat_axis=0, tiled=True)
    picked = (
        returned.reshape(-1, model_width)[target]
        .astype(jnp.float32)
        .reshape(tok_count, 2, model_width)
    )
    result = mixed_sum + jnp.sum(picked * route_weight[0][..., None], axis=1)
    return result.astype(jnp.bfloat16)[None]


def solution(mesh):
    in_specs = (
        P("dp", "sp", None, None),
        P("dp", "sp", None, None),
        P("dp", "sp", None, None),
        P(),
        P(),
        P("sp", "dp"),
        P("dp", "sp", None),
        P(),
        P("sp", None, None),
        P("sp", None, None),
        P("sp", None, None),
        P("dp", "sp", None),
        P("dp", "sp", None),
    )
    out_specs = P("dp", "sp", None)
    return jax.shard_map(
        on_device, mesh=mesh, in_specs=in_specs, out_specs=out_specs, check_vma=False
    )
```

profile of v0, /device:TPU:0, one launch (start us, length us, event | category | flops | bytes accessed | tf_op | source)
XLA Modules:
  0.0 305.6 jit_solution(6616813318897419317)
XLA Ops:
  6.6 1.1 fusion.41
  7.7 1.1 fusion.42
  8.8 0.5 multiply_cosine_fusion.1
  10.3 0.9 broadcast_in_dim.14
  11.2 7.3 %all-to-all-start.1 = ((bf16[128,16,128]{2,0,1:T(8,128)(2,1)}), bf16[128,16,128]{2,0,1:T(8,128)(2,1)S(1)}, u32[]{:S(2)}, u32[]{:S(2)}) async-start(bf16[128,16,128]{2,0,1:T(8,128)(2,1)} %bitcast.12), calls=%async_computation.1 | async-start | bytes 1048576 | tf_op jit(solution)/shard_map/all_to_all | solution.py:114
  19.2 0.9 subtract_convert_fusion.1
  20.1 1.5 pad_maximum_fusion
  21.6 11.4 %all-to-all-done.1 = bf16[128,16,128]{2,0,1:T(8,128)(2,1)S(1)} async-done(((bf16[128,16,128]{2,0,1:T(8,128)(2,1)}), bf16[128,16,128]{2,0,1:T(8,128)(2,1)S(1)}, u32[]{:S(2)}, u32[]{:S(2)}) %all-to-all-start.1) | async-done | bytes 524320 | tf_op jit(solution)/shard_map/all_to_all | solution.py:114
  33.0 3.6 %all-to-all-start = ((bf16[128,16,128]{2,0,1:T(8,128)(2,1)}), bf16[128,16,128]{2,0,1:T(8,128)(2,1)S(1)}, u32[]{:S(2)}, u32[]{:S(2)}) async-start(bf16[128,16,128]{2,0,1:T(8,128)(2,1)} %pad_maximum_fusion), calls=%async_computation | async-start | bytes 1048576 | tf_op jit(solution)/shard_map/all_to_all | solution.py:113
  36.7 14.6 %all-to-all-done = bf16[128,16,128]{2,0,1:T(8,128)(2,1)S(1)} async-done(((bf16[128,16,128]{2,0,1:T(8,128)(2,1)}), bf16[128,16,128]{2,0,1:T(8,128)(2,1)S(1)}, u32[]{:S(2)}, u32[]{:S(2)}) %all-to-all-start) | async-done | bytes 524320 | tf_op jit(solution)/shard_map/all_to_all | solution.py:113
  51.3 0.9 broadcast_in_dim.15
  52.2 3.6 %all-to-all-start.2 = ((bf16[128,16,128]{2,0,1:T(8,128)(2,1)}), bf16[128,16,128]{2,0,1:T(8,128)(2,1)S(1)}, u32[]{:S(2)}, u32[]{:S(2)}) async-start(bf16[128,16,128]{2,0,1:T(8,128)(2,1)} %bitcast.18), calls=%async_computation.2 | async-start | bytes 1048576 | tf_op jit(solution)/shard_map/all_to_all | solution.py:117
  55.9 0.7 all-gather.5.cloned.1.call-update
  56.8 13.7 %all-to-all-done.2 = bf16[128,16,128]{2,0,1:T(8,128)(2,1)S(1)} async-done(((bf16[128,16,128]{2,0,1:T(8,128)(2,1)}), bf16[128,16,128]{2,0,1:T(8,128)(2,1)S(1)}, u32[]{:S(2)}, u32[]{:S(2)}) %all-to-all-start.2) | async-done | bytes 524320 | tf_op jit(solution)/shard_map/all_to_all | solution.py:117
  70.6 3.4 %while.20 = (s32[]{:T(128)}, bf16[2,512,128]{2,1,0:T(8,128)(2,1)S(1)}, bf16[2,512,128]{2,1,0:T(8,128)(2,1)S(1)}, bf16[1024,128]{1,0:T(8,128)(2,1)S(1)}, bf16[1024,128]{1,0:T(8,128)(2,1)S(1)}, /*index=5*/s32[]{:T(128)}) while((s32[]{:T(128)}, bf16[2,512,128]{2,1,0:T(8,128)(2,1)S(1)}, bf16[2,512,128]{2,1,0:T(8,128)(2,1)S(1)}, ...), condition=%wide.region_5.6_spmd, body=%wide.region_2.5_spmd.sunk | while | flops 273218560 | bytes 7088205 | solution.py:73
  71.2 0.5 fusion.65
  71.7 0.7 fusion.66
  72.4 0.5 multiply_reduce_fusion.6
  72.9 0.5 fusion.65
  73.4 0.7 fusion.66
  74.1 3.5 %while.21 = (s32[]{:T(128)}, bf16[2,512,128]{2,1,0:T(8,128)(2,1)S(1)}, bf16[2,512,128]{2,1,0:T(8,128)(2,1)S(1)}, bf16[1024,128]{1,0:T(8,128)(2,1)S(1)}, bf16[1024,128]{1,0:T(8,128)(2,1)S(1)}, /*index=5*/s32[]{:T(128)}) while((s32[]{:T(128)}, bf16[2,512,128]{2,1,0:T(8,128)(2,1)S(1)}, bf16[2,512,128]{2,1,0:T(8,128)(2,1)S(1)}, ...), condition=%wide.region_9.10_spmd, body=%wide.region_6.9_spmd.sunk | while | flops 273218560 | bytes 7088205 | solution.py:73
  74.1 0.5 multiply_reduce_fusion.7
  74.7 0.5 fusion.69
  75.2 0.7 fusion.70
  75.9 0.5 multiply_reduce_fusion.7
  76.4 0.5 fusion.69
  76.9 0.7 fusion.70
  77.7 0.5 copy.114
  78.2 28.0 %all_to_all.88 = bf16[1024,2,128]{2,1,0:T(2,128)(2,1)S(1)} all-to-all(bf16[1024,2,128]{2,1,0:T(2,128)(2,1)S(1)} %copy.114), channel_id=1, replica_groups=mesh['sp'=8,'dp'=4] {'sp'}, dimensions={0} | all-to-all | bytes 1048576 | tf_op jit(solution)/shard_map/all_to_all | solution.py:126
  106.6 1.0 copy.117
  108.6 5.1 %all-gather.5.cloned.1.call-done = bf16[2048,512]{1,0:T(8,128)(2,1)} async-done(((bf16[256,512]{1,0:T(8,128)(2,1)}), bf16[2048,512]{1,0:T(8,128)(2,1)}) %all-gather.5.cloned.1.call-update) | async-done | bytes 2097168 | tf_op jit(solution)/shard_map/all_gather | solution.py:79
  113.7 23.2 %all-gather.3.cloned.1.call-done = bf16[4,128,2048]{2,1,0:T(8,128)(2,1)} async-done(((bf16[1,128,2048]{2,1,0:T(8,128)(2,1)}), bf16[4,128,2048]{2,1,0:T(8,128)(2,1)}) %all-gather.3.cloned.1.call-update) | async-done | bytes 2097168 | tf_op jit(solution)/shard_map/all_gather | solution.py:78
  136.9 4.3 %fusion.29 = bf16[4,128,512]{2,1,0:T(8,128)(2,1)} fusion(bf16[4,128,2048]{2,1,0:T(8,128)(2,1)} %all-gather.3.cloned.1.call-done, bf16[2048,512]{1,0:T(8,128)(2,1)} %all-gather.5.cloned.1.call-done), kind=kOutput, calls=%fused_computation.41 | convolution fusion | flops 1074003968 | bytes 4718592 | tf_op jit(solution)/shard_map/std,dc->stc/dot_general | solution.py:80
  141.1 3.7 %all-to-all-start.4 = ((bf16[4,128,512]{2,1,0:T(8,128)(2,1)}), bf16[4,128,512]{2,1,0:T(8,128)(2,1)S(1)}, u32[]{:S(2)}, u32[]{:S(2)}) async-start(bf16[4,128,512]{2,1,0:T(8,128)(2,1)} %fusion.29), calls=%async_computation.4 | async-start | bytes 1048576 | tf_op jit(solution)/shard_map/all_to_all | solution.py:83
  144.9 8.5 %all-to-all-done.4 = bf16[4,128,512]{2,1,0:T(8,128)(2,1)S(1)} async-done(((bf16[4,128,512]{2,1,0:T(8,128)(2,1)}), bf16[4,128,512]{2,1,0:T(8,128)(2,1)S(1)}, u32[]{:S(2)}, u32[]{:S(2)}) %all-to-all-start.4) | async-done | bytes 524320 | tf_op jit(solution)/shard_map/all_to_all | solution.py:83
  155.0 0.6 broadcast_in_dim.17
  155.6 1.2 reshape.305
  156.9 3.5 %scatter_custom_fusion = bf16[512,2048]{1,0:T(8,128)(2,1)S(1)} fusion(s32[256]{0:T(256)S(1)} %bitcast.142, bf16[256,2048]{1,0:T(8,128)(2,1)} %reshape.305, bf16[]{:T(256)} %constant.89.clone.1), kind=kCustom, calls=%fused_computation.50 | custom fusion | bytes 2097664 | tf_op jit(solution)/shard_map/scatter | solution.py:148
  160.4 53.4 %all_to_all.89 = bf16[8,64,2048]{2,1,0:T(8,128)(2,1)} all-to-all(bf16[8,64,2048]{2,1,0:T(8,128)(2,1)S(1)} %bitcast.127), channel_id=1, replica_groups=mesh['sp'=8,'dp'=4] {'sp'}, dimensions={0} | all-to-all | bytes 4194304 | tf_op jit(solution)/shard_map/all_to_all | solution.py:151
  213.8 9.5 %fusion.20 = f32[512,1792]{1,0:T(8,128)} fusion(bf16[512,2048]{1,0:T(8,128)(2,1)} %bitcast.41, bf16[1,2048,1792]{2,1,0:T(8,128)(2,1)} %param.25), kind=kOutput, calls=%fused_computation.30 | convolution fusion | flops 3758096384 | bytes 13107200 | tf_op jit(solution)/shard_map/dot_general | solution.py:154
  223.3 17.0 %fusion.24 = bf16[512,2048]{1,0:T(8,128)(2,1)} fusion(bf16[1,1792,2048]{2,1,0:T(8,128)(2,1)} %param.27, f32[512,1792]{1,0:T(8,128)} %fusion.20, bf16[512,2048]{1,0:T(8,128)(2,1)} %bitcast.41, bf16[1,2048,1792]{2,1,0:T(8,128)(2,1)} %param.26), kind=kOutput, calls=%fused_computation.33 | convolution fusion | flops 7522746368 | bytes 22544384 | tf_op jit(solution)/shard_map/dot_general | solution.py:157
  240.3 4.0 %all-to-all-start.6 = ((bf16[8,64,2048]{2,1,0:T(8,128)(2,1)}), bf16[8,64,2048]{2,1,0:T(8,128)(2,1)S(1)}, u32[]{:S(2)}, u32[]{:S(2)}) async-start(bf16[8,64,2048]{2,1,0:T(8,128)(2,1)} %bitcast.130), calls=%async_computation.6 | async-start | bytes 4194304 | tf_op jit(solution)/shard_map/all_to_all | solution.py:161
  244.4 1.3 copy.119
  245.7 46.2 %all-to-all-done.6 = bf16[8,64,2048]{2,1,0:T(8,128)(2,1)S(1)} async-done(((bf16[8,64,2048]{2,1,0:T(8,128)(2,1)}), bf16[8,64,2048]{2,1,0:T(8,128)(2,1)S(1)}, u32[]{:S(2)}, u32[]{:S(2)}) %all-to-all-start.6) | async-done | bytes 2097184 | tf_op jit(solution)/shard_map/all_to_all | solution.py:161
  291.9 1.4 gather_fusion
  293.3 1.3 reshape.290
  294.6 3.2 %multiply_reduce_fusion.2 = f32[128,2048]{1,0:T(8,128)S(1)} fusion(f32[128,2,2048]{2,1,0:T(2,128)S(1)} %reshape.290, f32[128,2]{1,0:T(8,128)S(1)} %copy.124), kind=kLoop, calls=%fused_computation.36 | loop fusion | flops 786432 | bytes 3146752 | tf_op jit(solution)/shard_map/reduce_sum | solution.py:167
  297.8 1.0 fusion.35
  (62 shorter events, 5.8 us)
Async XLA Ops:
  9.4 9.1 %copy-start.3 = (bf16[1,128,16,128]{3,2,1,0:T(8,128)(2,1)S(1)}, bf16[1,128,16,128]{3,2,1,0:T(8,128)(2,1)}, u32[]{:S(2)}) copy-start(bf16[1,128,16,128]{3,2,1,0:T(8,128)(2,1)} %param.17) | copy-start | bytes 1572868
  9.4 9.5 %copy-start.8 = (f32[128]{0:T(128)S(1)}, f32[128]{0:T(128)}, u32[]{:S(2)}) copy-start(f32[128]{0:T(128)} %param.20) | copy-start | bytes 1540
  11.2 21.8 %all-to-all-start.1 = ((bf16[128,16,128]{2,0,1:T(8,128)(2,1)}), bf16[128,16,128]{2,0,1:T(8,128)(2,1)S(1)}, u32[]{:S(2)}, u32[]{:S(2)}) async-start(bf16[128,16,128]{2,0,1:T(8,128)(2,1)} %bitcast.12), calls=%async_computation.1 | async-start | bytes 1048576 | tf_op jit(solution)/shard_map/all_to_all | solution.py:114
  20.1 16.5 %copy-start.4 = (bf16[1,128,4,128]{3,2,1,0:T(4,128)(2,1)S(1)}, bf16[1,128,4,128]{3,2,1,0:T(4,128)(2,1)}, u32[]{:S(2)}) copy-start(bf16[1,128,4,128]{3,2,1,0:T(4,128)(2,1)} %param.19) | copy-start | bytes 393220
  33.0 18.3 %all-to-all-start = ((bf16[128,16,128]{2,0,1:T(8,128)(2,1)}), bf16[128,16,128]{2,0,1:T(8,128)(2,1)S(1)}, u32[]{:S(2)}, u32[]{:S(2)}) async-start(bf16[128,16,128]{2,0,1:T(8,128)(2,1)} %pad_maximum_fusion), calls=%async_computation | async-start | bytes 1048576 | tf_op jit(solution)/shard_map/all_to_all | solution.py:113
  52.2 18.3 %all-to-all-start.2 = ((bf16[128,16,128]{2,0,1:T(8,128)(2,1)}), bf16[128,16,128]{2,0,1:T(8,128)(2,1)S(1)}, u32[]{:S(2)}, u32[]{:S(2)}) async-start(bf16[128,16,128]{2,0,1:T(8,128)(2,1)} %bitcast.18), calls=%async_computation.2 | async-start | bytes 1048576 | tf_op jit(solution)/shard_map/all_to_all | solution.py:117
  55.8 57.9 %all-gather.5.cloned.1.call-start = ((), (), s32[]{:S(2)}) async-start(), calls=%async_computation.8 | async-start | bytes 2359296 | tf_op jit(solution)/shard_map/all_gather | solution.py:79
  56.6 80.3 %all-gather.3.cloned.1.call-start = ((), (), s32[]{:S(2)}) async-start(), calls=%async_computation.7 | async-start | bytes 2621440 | tf_op jit(solution)/shard_map/all_gather | solution.py:78
  106.2 1.4 copy-start.6
  141.1 12.3 %all-to-all-start.4 = ((bf16[4,128,512]{2,1,0:T(8,128)(2,1)}), bf16[4,128,512]{2,1,0:T(8,128)(2,1)S(1)}, u32[]{:S(2)}, u32[]{:S(2)}) async-start(bf16[4,128,512]{2,1,0:T(8,128)(2,1)} %fusion.29), calls=%async_computation.4 | async-start | bytes 1048576 | tf_op jit(solution)/shard_map/all_to_all | solution.py:83
  153.5 1.0 copy-start
  153.9 0.9 copy-start.5
  240.3 4.0 %copy-start.7 = (f32[1,128,2]{1,2,0:T(2,128)S(1)}, f32[1,128,2]{1,2,0:T(2,128)}, u32[]{:S(2)}) copy-start(f32[1,128,2]{1,2,0:T(2,128)} %param.29) | copy-start | bytes 3076
  240.3 51.6 %all-to-all-start.6 = ((bf16[8,64,2048]{2,1,0:T(8,128)(2,1)}), bf16[8,64,2048]{2,1,0:T(8,128)(2,1)S(1)}, u32[]{:S(2)}, u32[]{:S(2)}) async-start(bf16[8,64,2048]{2,1,0:T(8,128)(2,1)} %bitcast.130), calls=%async_computation.6 | async-start | bytes 4194304 | tf_op jit(solution)/shard_map/all_to_all | solution.py:161
  294.6 3.2 %copy-start.1 = (bf16[1,128,2048]{2,1,0:T(8,128)(2,1)S(1)}, bf16[1,128,2048]{2,1,0:T(8,128)(2,1)}, u32[]{:S(2)}) copy-start(bf16[1,128,2048]{2,1,0:T(8,128)(2,1)} %param.23) | copy-start | bytes 1572868
  294.6 3.2 %copy-start.2 = (f32[1,128,2048]{2,1,0:T(8,128)S(1)}, f32[1,128,2048]{2,1,0:T(8,128)}, u32[]{:S(2)}) copy-start(f32[1,128,2048]{2,1,0:T(8,128)} %copy.119) | copy-start | bytes 3145732
Sparse Core Ops, SparseCore 0:
  58.8 54.8 all-gather.4
  115.2 21.5 all-gather.2
where the time goes:
time: 306 us
  waiting for transfers between devices  123 us (40%)
  blocking collectives  81.4 us (27%)
  matrix products  35.4 us (12%)
  starting transfers between devices  22.2 us (7%)
  local copies, waits for them, and re-layouts  15.1 us (5%)
  other arithmetic  14.2 us (5%)
  between operations  13.8 us (5%)
    all_to_all x1, blocking collectives, on_device(): lax.all_to_all(buffer, 'sp', split_axis=0, concat_axis=0, tiled=True)  53.4 us
    all_to_all x1, waiting for transfers between devices, on_device(): lax.all_to_all(served, 'sp', split_axis=0, concat_axis=0, tiled=True)  46.2 us
    all_to_all x1, blocking collectives, on_device(): lax.all_to_all(by_heads, 'sp', split_axis=0, concat_axis=1, tiled=True)  28 us
    all_gather x1, waiting for transfers between devices, project_tokens(): all_rows = lax.all_gather(attended[None], 'dp', axis=0, tiled=True)  23.2 us
    dot_general x1, matrix products, on_device(): jnp.dot(hidden, expert_down[0], preferred_element_type=jnp.float32)  17 us
    all_to_all x1, waiting for transfers between devices, on_device(): lax.all_to_all(rot_query, 'sp', split_axis=1, concat_axis=0, tiled=True)  14.6 us
    all_to_all x1, waiting for transfers between devices, on_device(): lax.all_to_all(jnp.repeat(value_rows, group_size, axis=1), 'sp', split_ax...  13.7 us
    all_to_all x1, waiting for transfers between devices, on_device(): lax.all_to_all(jnp.repeat(rot_key, group_size, axis=1), 'sp', split_axis=...  11.4 us
  transfers between devices with their start and end apart: 7, of which 7 were waited for; matrix products, arithmetic and copies ran while one was open for 5% of the time, Pallas kernels for 0%

commit v1 on v0

v1 whole, which is shorter than its diff:
```python
import jax
import jax.numpy as jnp
from jax import lax
from jax.experimental import pallas as pl
from jax.experimental.pallas import tpu as pltpu
from jax.sharding import PartitionSpec as P

GRID_W = 64
EPS = 1e-06
THETA = 10000.0
F32 = jnp.float32
BF16 = jnp.bfloat16


def swap(array, axis, bits):
    size = lax.axis_size(axis)
    return lax.ppermute(array, axis, [(i, i ^ bits) for i in range(size)])


def angle_tables(positions, width):
    lane = jnp.arange(width, dtype=jnp.int32)
    half = width // 2
    quarter = half // 2
    inverse = THETA ** (-(lane % quarter).astype(F32) / quarter)
    place = jnp.where(
        lane[None, :] < half, (positions // GRID_W)[:, None], (positions % GRID_W)[:, None]
    ).astype(F32)
    angles = place * inverse[None, :]
    sign = jnp.where((lane % half) < quarter, -1.0, 1.0)
    return jnp.cos(angles), jnp.sin(angles) * sign[None, :]


def pack_rows(queries, keys, values, query_gain, key_gain, cosine, sine, parts):
    rows, query_width = queries.shape
    width = cosine.shape[1]
    heads = query_width // width
    kv_heads = keys.shape[1] // width
    group = heads // kv_heads
    per = heads // parts
    kv_per = max(1, per // group)
    block = (per + 2 * kv_per) * width

    def body(q_ref, k_ref, v_ref, qg_ref, kg_ref, c_ref, s_ref, o_ref):
        lane = lax.broadcasted_iota(jnp.int32, (rows, width), 1)
        low = (lane % (width // 2)) < (width // 4)
        cos = c_ref[...]
        sin = s_ref[...]

        def turned(part, gain):
            x = part.astype(F32)
            a = x * lax.rsqrt(jnp.mean(x * x, axis=-1, keepdims=True) + EPS) * gain
            other = jnp.where(
                low, pltpu.roll(a, width - width // 4, 1), pltpu.roll(a, width // 4, 1)
            )
            return (a * cos + other * sin).astype(BF16)

        for head in range(heads):
            at = (head % per) * width
            o_ref[head // per, :, at : at + width] = turned(
                q_ref[:, head * width : (head + 1) * width], qg_ref[...]
            )
        turned_keys = [
            turned(k_ref[:, h * width : (h + 1) * width], kg_ref[...]) for h in range(kv_heads)
        ]
        for part in range(parts):
            for i in range(kv_per):
                h = (part * per) // group + i
                at = (per + i) * width
                o_ref[part, :, at : at + width] = turned_keys[h]
                at = (per + kv_per + i) * width
                o_ref[part, :, at : at + width] = v_ref[:, h * width : (h + 1) * width]

    return pl.pallas_call(
        body, out_shape=jax.ShapeDtypeStruct((parts, rows, block), BF16), name="pack_rows"
    )(queries, keys, values, query_gain[None], key_gain[None], cosine, sine)


def attend(packed, per, kv_per, width):
    length, full = packed.shape
    rows = min(256, length)

    def body(q_ref, all_ref, o_ref):
        for head in range(per):
            kv = head * kv_per // per
            q = q_ref[:, head * width : (head + 1) * width]
            k = all_ref[:, (per + kv) * width : (per + kv + 1) * width]
            v = all_ref[:, (per + kv_per + kv) * width : (per + kv_per + kv + 1) * width]
            scores = lax.dot_general(
                q, k, (((1,), (1,)), ((), ())), preferred_element_type=F32
            ) * width ** (-0.5)
            e = jnp.exp(scores - jnp.max(scores, axis=-1, keepdims=True))
            weights = (e * (1.0 / jnp.sum(e, axis=-1, keepdims=True))).astype(BF16)
            o_ref[:, head * width : (head + 1) * width] = jnp.dot(
                weights, v, preferred_element_type=F32
            ).astype(BF16)

    return pl.pallas_call(
        body,
        grid=(length // rows,),
        in_specs=[
            pl.BlockSpec((rows, full), lambda i: (i, 0)),
            pl.BlockSpec((length, full), lambda i: (0, 0)),
        ],
        out_specs=pl.BlockSpec((rows, per * width), lambda i: (i, 0)),
        out_shape=jax.ShapeDtypeStruct((length, per * width), BF16),
        name="attend",
    )(packed, packed)


def expert_rows(blocks, gate, up, down):
    count = len(blocks)
    rows, model = blocks[0].shape
    hidden_width = gate.shape[1]
    tile = 256
    steps = hidden_width // tile

    def body(*refs):
        x_refs = refs[:count]
        g_ref, u_ref, d_ref = refs[count : count + 3]
        o_refs = refs[count + 3 : 2 * count + 3]
        x_all, acc = refs[2 * count + 3 :]
        step = pl.program_id(0)

        @pl.when(step == 0)
        def _():
            for i in range(count):
                x_all[i * rows : (i + 1) * rows, :] = x_refs[i][...]

        x = x_all[...]
        g = jnp.dot(x, g_ref[...], preferred_element_type=F32)
        u = jnp.dot(x, u_ref[...], preferred_element_type=F32)
        hidden = (g / (1.0 + jnp.exp(-g)) * u).astype(BF16)
        y = jnp.dot(hidden, d_ref[...], preferred_element_type=F32)

        @pl.when(step == 0)
        def _():
            acc[...] = y

        @pl.when(step > 0)
        def _():
            acc[...] += y

        @pl.when(step == steps - 1)
        def _():
            for i in range(count):
                o_refs[i][...] = acc[i * rows : (i + 1) * rows, :].astype(BF16)

    whole = pl.BlockSpec((rows, model), lambda i: (0, 0))
    return pl.pallas_call(
        body,
        grid=(steps,),
        in_specs=[whole] * count
        + [
            pl.BlockSpec((model, tile), lambda i: (0, i)),
            pl.BlockSpec((model, tile), lambda i: (0, i)),
            pl.BlockSpec((tile, model), lambda i: (i, 0)),
        ],
        out_specs=[whole] * count,
        out_shape=[jax.ShapeDtypeStruct((rows, model), BF16)] * count,
        scratch_shapes=[
            pltpu.VMEM((count * rows, model), BF16),
            pltpu.VMEM((count * rows, model), F32),
        ],
        name="expert_rows",
    )(*blocks, gate, up, down)


def slots_of(chosen, capacity, experts):
    tokens = chosen.shape[0]
    by_block = chosen.reshape(2, tokens)
    onehot = (by_block[..., None] == jnp.arange(experts, dtype=jnp.int32)).astype(F32)
    earlier = (jnp.arange(tokens)[:, None] > jnp.arange(tokens)[None, :]).astype(F32)
    before = jnp.einsum("ij,bje->bie", earlier, onehot, preferred_element_type=F32)
    rank = jnp.sum(before * onehot, axis=-1).astype(jnp.int32)
    return (jnp.arange(2, dtype=jnp.int32)[:, None] * capacity + rank).reshape(tokens, 2)


def on_device(
    queries, key_rows, values, query_gain, key_gain, out_weight, residual, norm_gain,
    expert_gate, expert_up, expert_down, routes, route_weight,
):
    parts = lax.axis_size("sp")
    columns = lax.axis_size("dp")
    me = lax.axis_index("sp")
    _, tokens, heads, width = queries.shape
    kv_heads = key_rows.shape[2]
    group = heads // kv_heads
    per = heads // parts
    kv_per = max(1, per // group)
    model = residual.shape[-1]
    half = parts // 2
    near = parts // 4

    positions = me * tokens + jnp.arange(tokens, dtype=jnp.int32)
    cosine, sine = angle_tables(positions, width)
    packed = pack_rows(
        queries.reshape(tokens, heads * width),
        key_rows.reshape(tokens, kv_heads * width),
        values.reshape(tokens, kv_heads * width),
        query_gain, key_gain, cosine, sine, parts,
    )
    by_head = lax.all_to_all(packed, "sp", split_axis=0, concat_axis=0, tiled=True)

    shards = [None] * parts
    for far in range(4):
        shard = out_weight if far == 0 else swap(out_weight, "sp", far * near)
        shards[far * near] = shard
        for close in range(1, near):
            shards[far * near + close] = swap(shard, "sp", close)
    own_columns = jnp.concatenate(shards, axis=0)
    core_columns = swap(own_columns, "dp", 1)

    experts = expert_gate.shape[0] * parts
    capacity = max(2, 4 * (tokens // 2) // experts)
    slots = 2 * capacity
    chosen = routes[0]
    slot = slots_of(chosen, capacity, experts)
    weight = route_weight[0]
    chosen_far = swap(chosen, "sp", half)
    slot_far = swap(slot, "sp", half)
    weight_far = swap(weight, "sp", half)
    place = jnp.arange(half * slots, dtype=jnp.int32)
    place_expert = me ^ (place // slots)
    place_slot = place % slots

    def selection(chosen, slot):
        return [
            (chosen[:, j, None] == place_expert[None]) & (slot[:, j, None] == place_slot[None])
            for j in range(2)
        ]

    pick = selection(chosen, slot)
    pick_far = selection(chosen_far, slot_far)

    attended = attend(by_head.reshape(parts * tokens, -1), per, kv_per, width)
    returned = lax.all_to_all(
        attended.reshape(parts, tokens, per * width), "sp", split_axis=0, concat_axis=0, tiled=True
    )
    rows = jnp.concatenate(
        [lax.dynamic_index_in_dim(returned, me ^ k, 0, keepdims=False) for k in range(parts)],
        axis=1,
    )

    chips = columns // 2
    gathered = jnp.concatenate([rows] + [swap(rows, "dp", 2 * k) for k in range(1, chips)], axis=0)
    mine = jnp.dot(gathered, own_columns, preferred_element_type=F32).astype(BF16)
    other = jnp.dot(gathered, core_columns, preferred_element_type=F32).astype(BF16)
    first = lax.axis_index("dp") % 2 == 0
    both = jnp.concatenate(
        [jnp.where(first, mine, other), jnp.where(first, other, mine)], axis=1
    ).reshape(chips, tokens, -1)
    back = [both[0]] + [swap(both[k], "dp", 2 * k) for k in range(1, chips)]
    chip = lax.axis_index("dp") // 2
    if chips == 2:
        ordered = [jnp.where(chip == 0, back[0], back[1]), jnp.where(chip == 0, back[1], back[0])]
    else:
        stacked = jnp.stack(back)
        ordered = [
            lax.dynamic_index_in_dim(stacked, chip ^ k, 0, keepdims=False) for k in range(chips)
        ]
    projected = jnp.concatenate(ordered, axis=1).astype(F32)
    mixed_sum = residual[0].astype(F32) + projected
    normed = (
        mixed_sum
        * lax.rsqrt(jnp.mean(mixed_sum * mixed_sum, axis=-1, keepdims=True) + EPS)
        * norm_gain
    ).astype(BF16)

    normed_far = swap(normed, "sp", half)

    def serve(source, picks):
        chosen_rows = (picks[0] | picks[1]).astype(BF16)
        sent = lax.dot_general(
            chosen_rows, source, (((0,), (0,)), ((), ())), preferred_element_type=F32
        ).astype(BF16)
        blocks = [sent[k * slots : (k + 1) * slots] for k in range(half)]
        blocks = [blocks[0]] + [swap(blocks[k], "sp", k) for k in range(1, half)]
        results = expert_rows(blocks, expert_gate[0], expert_up[0], expert_down[0])
        return [results[0]] + [swap(results[k], "sp", k) for k in range(1, half)]

    def combine(results, picks, weight):
        flat = jnp.concatenate(results, axis=0)
        return sum(
            jnp.dot(picks[j].astype(BF16), flat, preferred_element_type=F32) * weight[:, j, None]
            for j in range(2)
        )

    near_results = serve(normed, pick)
    far_results = serve(normed_far, pick_far)
    crossed = swap(combine(far_results, pick_far, weight_far).astype(BF16), "sp", half)
    result = mixed_sum + combine(near_results, pick, weight) + crossed.astype(F32)
    return result.astype(BF16)[None]


def solution(mesh):
    in_specs = (
        P("dp", "sp", None, None),
        P("dp", "sp", None, None),
        P("dp", "sp", None, None),
        P(),
        P(),
        P("sp", "dp"),
        P("dp", "sp", None),
        P(),
        P("sp", None, None),
        P("sp", None, None),
        P("sp", None, None),
        P("dp", "sp", None),
        P("dp", "sp", None),
    )
    out_specs = P("dp", "sp", None)
    return jax.shard_map(
        on_device, mesh=mesh, in_specs=in_specs, out_specs=out_specs, check_vma=False
    )
```

time: 306 us -> 229 us (0.75)
  blocking collectives: 81.4 us -> 0 us
  Pallas kernels: 0 us -> 41.9 us
  matrix products: 35.4 us -> 8.38 us
  starting transfers between devices: 22.2 us -> 45.2 us
  between operations: 13.8 us -> 0.38 us
  other arithmetic: 14.2 us -> 1.71 us
  waiting for transfers between devices: 123 us -> 114 us
    ppermute x0 -> x27, waiting for transfers between devices: none -> 103 us  [swap(): return lax.ppermute(array, axis, [(i, i ^ bits) for i in range(size)])]
    all_to_all x5 -> x2, waiting for transfers between devices: 94.5 us -> 11.4 us  [the longest x1 11.4 us: on_device(): lax.all_to_all(attended.reshape(parts, tokens, per * width), 'sp', split_...]
    all_to_all x2 -> x0, blocking collectives: 81.4 us -> none  [the longest x1 53.4 us: on_device(): lax.all_to_all(buffer, 'sp', split_axis=0, concat_axis=0, tiled=True)]
    pallas_call x0 -> x4, Pallas kernels: none -> 41.9 us  [the longest x2 29.2 us: expert_rows(): pl.pallas_call(body, grid=(steps,), in_specs=[whole] * count + [pl.BlockS...]
    ppermute x0 -> x27, starting transfers between devices: none -> 33.9 us  [swap(): return lax.ppermute(array, axis, [(i, i ^ bits) for i in range(size)])]
    all_gather x2 -> x0, waiting for transfers between devices: 28.3 us -> none  [the longest x1 23.2 us: project_tokens(): all_rows = lax.all_gather(attended[None], 'dp', axis=0, tiled=True)]
    dot_general x11 -> x9, matrix products: 35.4 us -> 8.38 us  [the longest x4 2.4 us: combine(): jnp.dot(picks[j].astype(BF16), flat, preferred_element_type=F32)]
    unnamed x19 -> x48, local copies, waits for them, and re-layouts: 0.51 us -> 11.7 us
  transfers between devices with their start and end apart: 7 -> 29, of which waited for: 7 -> 14; matrix products, arithmetic and copies ran while one was open for 5% -> 8% of each run, Pallas kernels for 0% -> 16%
where the time goes in v1:
time: 229 us; the launch traced here: 228 us
  waiting for transfers between devices  114 us (50%)
  starting transfers between devices  45.2 us (20%)
  Pallas kernels  41.9 us (18%)
  local copies, waits for them, and re-layouts  16.5 us (7%)
  matrix products  8.38 us (4%)
    ppermute x27, waiting for transfers between devices, swap(): return lax.ppermute(array, axis, [(i, i ^ bits) for i in range(size)])  103 us
    ppermute x27, starting transfers between devices, swap(): return lax.ppermute(array, axis, [(i, i ^ bits) for i in range(size)])  33.9 us
    pallas_call x2, Pallas kernels, expert_rows(): pl.pallas_call(body, grid=(steps,), in_specs=[whole] * count + [pl.BlockS...  29.2 us
    unnamed x48, local copies, waits for them, and re-layouts  11.7 us
    all_to_all x1, waiting for transfers between devices, on_device(): lax.all_to_all(attended.reshape(parts, tokens, per * width), 'sp', split_...  11.4 us
    pallas_call x1, Pallas kernels, attend(): pl.pallas_call(body, grid=(length // rows,), in_specs=[pl.BlockSpec((rows...  7.88 us
    all_to_all x1, starting transfers between devices, on_device(): lax.all_to_all(packed, 'sp', split_axis=0, concat_axis=0, tiled=True)  7.29 us
    pallas_call x1, Pallas kernels, pack_rows(): pl.pallas_call(body, out_shape=jax.ShapeDtypeStruct((parts, rows, block),...  4.86 us
  transfers between devices with their start and end apart: 29, of which 14 were waited for; matrix products, arithmetic and copies ran while one was open for 8% of the time, Pallas kernels for 16%

profile of v1, /device:TPU:0, one launch (start us, length us, event | category | flops | bytes accessed | tf_op | source)
XLA Modules:
  0.0 228.5 jit_solution(10935398655574518280)
XLA Ops:
  0.0 2.0 copy.22
  2.0 1.7 copy_bitcast_fusion.1
  3.7 1.0 sine_multiply_fusion
  4.7 4.9 %pack_rows.1 = bf16[8,128,512]{2,1,0:T(8,128)(2,1)} custom-call(bf16[128,2048]{1,0:T(8,128)(2,1)} %bitcast.87, bf16[128,512]{1,0:T(8,128)(2,1)} %get-tuple-element.54.k_ref, bf16[128,512]{1,0:T(8,128)(2,1)} %get-tuple-element.53.v_ref, f32[1,128]{1,0:T(1,128)} %bitcast.95, f32[1,128]{1,0:T(1,128)} %bitcast.96, f32[128,128]{1,0:T(8,128)} %get-tuple-element.38.c_ref, ...), custom_call_target="tpu_custom_call" | custom-call | tf_op jit(solution)/shard_map/pack_rows/pallas_call | solution.py:73
  9.5 7.3 %all-to-all-start = ((bf16[8,128,512]{2,1,0:T(8,128)(2,1)}), bf16[8,128,512]{2,1,0:T(8,128)(2,1)S(1)}, u32[]{:S(2)}, u32[]{:S(2)}) async-start(bf16[8,128,512]{2,1,0:T(8,128)(2,1)} %pack_rows.1), calls=%async_computation | async-start | bytes 2097152 | tf_op jit(solution)/shard_map/all_to_all | solution.py:202
  16.8 2.0 collective-permute-start.2
  18.9 2.4 %collective-permute-start.4 = (bf16[256,512]{1,0:T(8,128)(2,1)S(1)}, bf16[256,512]{1,0:T(8,128)(2,1)S(1)}, u32[]{:S(2)}, u32[]{:S(2)}) collective-permute-start(bf16[256,512]{1,0:T(8,128)(2,1)S(1)} %copy-done.8), channel_id=1, source_target_pairs={{0,16},{4,20},{8,24},{12,28},{16,0},{20,4},{24,8},{28,12},{1,17},{... | collective-permute-start | bytes 786440 | tf_op jit(solution)/shard_map/ppermute | solution.py:17
  21.2 1.5 collective-permute-start.1
  23.2 17.5 %collective-permute-done.2 = bf16[256,512]{1,0:T(8,128)(2,1)S(1)} collective-permute-done((bf16[256,512]{1,0:T(8,128)(2,1)S(1)}, bf16[256,512]{1,0:T(8,128)(2,1)S(1)}, u32[]{:S(2)}, u32[]{:S(2)}) %collective-permute-start.2) | collective-permute-done | bytes 262176 | tf_op jit(solution)/shard_map/ppermute | solution.py:17
  40.7 1.9 collective-permute-start.3
  43.4 17.4 %collective-permute-done.4 = bf16[256,512]{1,0:T(8,128)(2,1)S(1)} collective-permute-done((bf16[256,512]{1,0:T(8,128)(2,1)S(1)}, bf16[256,512]{1,0:T(8,128)(2,1)S(1)}, u32[]{:S(2)}, u32[]{:S(2)}) %collective-permute-start.4) | collective-permute-done | bytes 262176 | tf_op jit(solution)/shard_map/ppermute | solution.py:17
  60.8 1.1 collective-permute-start.5
  63.3 1.0 collective-permute-start.7
  65.7 1.0 copy-done
  66.7 7.9 %attend.1 = bf16[1024,256]{1,0:T(8,128)(2,1)} custom-call(bf16[1024,512]{1,0:T(8,128)(2,1)} %bitcast.84, bf16[1024,512]{1,0:T(8,128)(2,1)} %bitcast.85), custom_call_target="tpu_custom_call" | custom-call | tf_op jit(solution)/shard_map/attend/pallas_call | solution.py:97
  74.6 4.0 %all-to-all-start.1 = ((bf16[8,128,256]{2,1,0:T(8,128)(2,1)}), bf16[8,128,256]{2,1,0:T(8,128)(2,1)S(1)}, u32[]{:S(2)}, u32[]{:S(2)}) async-start(bf16[8,128,256]{2,1,0:T(8,128)(2,1)} %bitcast.86), calls=%async_computation.1 | async-start | bytes 1048576 | tf_op jit(solution)/shard_map/all_to_all | solution.py:236
  78.6 0.7 constant_dynamic-update-slice_fusion.2
  81.6 11.4 %all-to-all-done.1 = bf16[8,128,256]{2,1,0:T(8,128)(2,1)S(1)} async-done(((bf16[8,128,256]{2,1,0:T(8,128)(2,1)}), bf16[8,128,256]{2,1,0:T(8,128)(2,1)S(1)}, u32[]{:S(2)}, u32[]{:S(2)}) %all-to-all-start.1) | async-done | bytes 524320 | tf_op jit(solution)/shard_map/all_to_all | solution.py:236
  93.1 1.6 collective-permute-start
  95.1 2.7 %collective-permute-start.16 = (s32[128,2]{0,1:T(2,128)S(1)}, s32[128,2]{0,1:T(2,128)S(1)}, u32[]{:S(2)}, u32[]{:S(2)}) collective-permute-start(s32[128,2]{0,1:T(2,128)S(1)} %bitcast.91), channel_id=1, source_target_pairs={{0,16},{4,20},{8,24},{12,28},{16,0},{20,4},{24,8},{28,12},{1,17},{... | collective-permute-start | bytes 3080 | tf_op jit(solution)/shard_map/ppermute | solution.py:17
  98.0 7.5 %collective-permute-done = bf16[128,2048]{1,0:T(8,128)(2,1)S(1)} collective-permute-done((bf16[128,2048]{1,0:T(8,128)(2,1)S(1)}, bf16[128,2048]{1,0:T(8,128)(2,1)S(1)}, u32[]{:S(2)}, u32[]{:S(2)}) %collective-permute-start) | collective-permute-done | bytes 524320 | tf_op jit(solution)/shard_map/ppermute | solution.py:17
  105.5 2.3 %convolution_convert_fusion.2 = bf16[256,512]{1,0:T(8,128)(2,1)S(1)} fusion(bf16[2048,512]{1,0:T(8,128)(2,1)} %collective-permute-done.8, bf16[128,2048]{1,0:T(8,128)(2,1)S(1)} %collective-permute-done, bf16[128,2048]{1,0:T(8,128)(2,1)S(1)} %bitcast_dynamic-update-slice_fusion), kind=kOutput, calls=%fused_computation.13 | convolution fusion | flops 539099136 | bytes 3407872 | tf_op jit(solution)/shard_map/dot_general | solution.py:247
  107.9 2.3 %broadcast_select_fusion.1 = (bf16[256,512]{1,0:T(8,128)(2,1)S(1)}, bf16[256,512]{1,0:T(8,128)(2,1)S(1)}) fusion(bf16[256,512]{1,0:T(8,128)(2,1)S(1)} %convolution_convert_fusion.2, pred[]{:T(512)S(6)} %eq.145, bf16[2048,512]{1,0:T(8,128)(2,1)} %constant_dynamic-update-slice_fusion, bf16[128,2048]{1,0:T(8,128)(2,1)S(1)} %collective-permute-done, ...), kind=kOutput, calls=%fused_computation.29 | convolution fusion | flops 539361280 | bytes 3932161 | tf_op jit(solution)/shard_map/dot_general | solution.py:246
  110.2 1.6 collective-permute-start.9
  111.8 4.8 %collective-permute-done.9 = bf16[128,1024]{1,0:T(8,128)(2,1)S(1)} collective-permute-done((bf16[128,1024]{1,0:T(8,128)(2,1)S(1)}, bf16[128,1024]{1,0:T(8,128)(2,1)S(1)}, u32[]{:S(2)}, u32[]{:S(2)}) %collective-permute-start.9) | collective-permute-done | bytes 262176 | tf_op jit(solution)/shard_map/ppermute | solution.py:17
  117.3 2.4 %collective-permute-start.18 = (bf16[128,2048]{1,0:T(8,128)(2,1)S(1)}, bf16[128,2048]{1,0:T(8,128)(2,1)S(1)}, u32[]{:S(2)}, u32[]{:S(2)}) collective-permute-start(bf16[128,2048]{1,0:T(8,128)(2,1)S(1)} %multiply_convert_fusion), channel_id=1, source_target_pairs={{0,16},{4,20},{8,24},{12,28},{16,0},{20,4},{24,8},{28,12},{1,17},{... | collective-permute-start | bytes 1572872 | tf_op jit(solution)/shard_map/ppermute | solution.py:17
  120.3 0.8 fusion.54
  121.1 3.6 %collective-permute-start.11 = (bf16[64,2048]{1,0:T(8,128)(2,1)S(1)}, bf16[64,2048]{1,0:T(8,128)(2,1)S(1)}, u32[]{:S(2)}, u32[]{:S(2)}) collective-permute-start(bf16[64,2048]{1,0:T(8,128)(2,1)S(1)} %get-tuple-element.30), channel_id=1, source_target_pairs={{0,8},{4,12},{8,0},{12,4},{16,24},{20,28},{24,16},{28,20},{1,9},{5... | collective-permute-start | bytes 786440 | tf_op jit(solution)/shard_map/ppermute | solution.py:17
  125.6 4.0 %collective-permute-done.10.refs_1_ = bf16[64,2048]{1,0:T(8,128)(2,1)S(1)} collective-permute-done((bf16[64,2048]{1,0:T(8,128)(2,1)S(1)}, bf16[64,2048]{1,0:T(8,128)(2,1)S(1)}, u32[]{:S(2)}, u32[]{:S(2)}) %collective-permute-start.10) | collective-permute-done | bytes 262176 | tf_op jit(solution)/shard_map/ppermute | solution.py:17
  129.6 12.7 %collective-permute-done.11.refs_2_ = bf16[64,2048]{1,0:T(8,128)(2,1)S(1)} collective-permute-done((bf16[64,2048]{1,0:T(8,128)(2,1)S(1)}, bf16[64,2048]{1,0:T(8,128)(2,1)S(1)}, u32[]{:S(2)}, u32[]{:S(2)}) %collective-permute-start.11) | collective-permute-done | bytes 262176 | tf_op jit(solution)/shard_map/ppermute | solution.py:17
  142.2 1.7 collective-permute-done.12.refs_3_
  144.6 14.6 %expert_rows.2 = (bf16[64,2048]{1,0:T(8,128)(2,1)}, bf16[64,2048]{1,0:T(8,128)(2,1)}, bf16[64,2048]{1,0:T(8,128)(2,1)}, bf16[64,2048]{1,0:T(8,128)(2,1)}) custom-call(bf16[64,2048]{1,0:T(8,128)(2,1)} %get-tuple-element.32.refs_0_, bf16[64,2048]{1,0:T(8,128)(2,1)} %copy-done.2, bf16[64,2048]{1,0:T(8,128)(2,1)} %copy-done.4, bf16[64,2048]{1,0:T(8,128)(2,1)} %copy-done.7, ...), custom_call_target="tpu_custom_call" | custom-call | tf_op jit(solution)/shard_map/expert_rows/pallas_call | solution.py:149
  159.3 3.1 %collective-permute-start.13 = (bf16[64,2048]{1,0:T(8,128)(2,1)}, bf16[64,2048]{1,0:T(8,128)(2,1)}, u32[]{:S(2)}, u32[]{:S(2)}) collective-permute-start(bf16[64,2048]{1,0:T(8,128)(2,1)} %get-tuple-element.14), channel_id=1, source_target_pairs={{0,4},{4,0},{8,12},{12,8},{16,20},{20,16},{24,28},{28,24},{1,5},{5... | collective-permute-start | bytes 786440 | tf_op jit(solution)/shard_map/ppermute | solution.py:17
  163.0 0.8 fusion.53
  163.9 3.4 %collective-permute-start.21 = (bf16[64,2048]{1,0:T(8,128)(2,1)S(1)}, bf16[64,2048]{1,0:T(8,128)(2,1)S(1)}, u32[]{:S(2)}, u32[]{:S(2)}) collective-permute-start(bf16[64,2048]{1,0:T(8,128)(2,1)S(1)} %get-tuple-element.25), channel_id=1, source_target_pairs={{0,12},{4,8},{8,4},{12,0},{16,28},{20,24},{24,20},{28,16},{1,13},{... | collective-permute-start | bytes 786440 | tf_op jit(solution)/shard_map/ppermute | solution.py:17
  167.4 10.9 %collective-permute-done.19.refs_1_ = bf16[64,2048]{1,0:T(8,128)(2,1)S(1)} collective-permute-done((bf16[64,2048]{1,0:T(8,128)(2,1)S(1)}, bf16[64,2048]{1,0:T(8,128)(2,1)S(1)}, u32[]{:S(2)}, u32[]{:S(2)}) %collective-permute-start.19) | collective-permute-done | bytes 262176 | tf_op jit(solution)/shard_map/ppermute | solution.py:17
  178.3 1.8 collective-permute-done.21.refs_3_
  180.8 14.6 %expert_rows.3 = (bf16[64,2048]{1,0:T(8,128)(2,1)}, bf16[64,2048]{1,0:T(8,128)(2,1)}, bf16[64,2048]{1,0:T(8,128)(2,1)}, bf16[64,2048]{1,0:T(8,128)(2,1)}) custom-call(bf16[64,2048]{1,0:T(8,128)(2,1)} %get-tuple-element.28.refs_0_, bf16[64,2048]{1,0:T(8,128)(2,1)} %copy-done.3, bf16[64,2048]{1,0:T(8,128)(2,1)} %copy-done.5, bf16[64,2048]{1,0:T(8,128)(2,1)} %copy-done.6, ...), custom_call_target="tpu_custom_call" | custom-call | tf_op jit(solution)/shard_map/expert_rows/pallas_call | solution.py:149
  195.4 1.0 collective-permute-start.22
  196.4 1.0 constant_dynamic-update-slice_fusion.10
  197.3 1.4 collective-permute-start.23
  198.8 1.0 constant_dynamic-update-slice_fusion.15
  199.7 1.5 collective-permute-start.24
  201.3 1.3 collective-permute-done.22
  202.6 2.4 %collective-permute-done.23 = bf16[64,2048]{1,0:T(8,128)(2,1)S(1)} collective-permute-done((bf16[64,2048]{1,0:T(8,128)(2,1)}, bf16[64,2048]{1,0:T(8,128)(2,1)S(1)}, u32[]{:S(2)}, u32[]{:S(2)}) %collective-permute-start.23) | collective-permute-done | bytes 262176 | tf_op jit(solution)/shard_map/ppermute | solution.py:17
  205.0 5.6 %collective-permute-done.24 = bf16[64,2048]{1,0:T(8,128)(2,1)S(1)} collective-permute-done((bf16[64,2048]{1,0:T(8,128)(2,1)}, bf16[64,2048]{1,0:T(8,128)(2,1)S(1)}, u32[]{:S(2)}, u32[]{:S(2)}) %collective-permute-start.24) | collective-permute-done | bytes 262176 | tf_op jit(solution)/shard_map/ppermute | solution.py:17
  211.9 15.2 %collective-permute-done.26 = bf16[128,2048]{1,0:T(8,128)(2,1)S(1)} collective-permute-done((bf16[128,2048]{1,0:T(8,128)(2,1)S(1)}, bf16[128,2048]{1,0:T(8,128)(2,1)S(1)}, u32[]{:S(2)}, u32[]{:S(2)}) %collective-permute-start.26) | collective-permute-done | bytes 524320 | tf_op jit(solution)/shard_map/ppermute | solution.py:17
  227.1 1.3 fusion.6
  (101 shorter events, 12.5 us)
Async XLA Ops:
  3.7 13.1 %copy-start.8 = (bf16[256,512]{1,0:T(8,128)(2,1)S(1)}, bf16[256,512]{1,0:T(8,128)(2,1)}, u32[]{:S(2)}) copy-start(bf16[256,512]{1,0:T(8,128)(2,1)} %param.18) | copy-start | bytes 786436
  9.5 56.2 %all-to-all-start = ((bf16[8,128,512]{2,1,0:T(8,128)(2,1)}), bf16[8,128,512]{2,1,0:T(8,128)(2,1)S(1)}, u32[]{:S(2)}, u32[]{:S(2)}) async-start(bf16[8,128,512]{2,1,0:T(8,128)(2,1)} %pack_rows.1), calls=%async_computation | async-start | bytes 2097152 | tf_op jit(solution)/shard_map/all_to_all | solution.py:202
  16.8 23.9 %collective-permute-start.2 = (bf16[256,512]{1,0:T(8,128)(2,1)S(1)}, bf16[256,512]{1,0:T(8,128)(2,1)S(1)}, u32[]{:S(2)}, u32[]{:S(2)}) collective-permute-start(bf16[256,512]{1,0:T(8,128)(2,1)S(1)} %copy-done.8), channel_id=1, source_target_pairs={{0,8},{4,12},{8,0},{12,4},{16,24},{20,28},{24,16},{28,20},{1,9},{5... | collective-permute-start | bytes 786440 | tf_op jit(solution)/shard_map/ppermute | solution.py:17
  18.9 42.0 %collective-permute-start.4 = (bf16[256,512]{1,0:T(8,128)(2,1)S(1)}, bf16[256,512]{1,0:T(8,128)(2,1)S(1)}, u32[]{:S(2)}, u32[]{:S(2)}) collective-permute-start(bf16[256,512]{1,0:T(8,128)(2,1)S(1)} %copy-done.8), channel_id=1, source_target_pairs={{0,16},{4,20},{8,24},{12,28},{16,0},{20,4},{24,8},{28,12},{1,17},{... | collective-permute-start | bytes 786440 | tf_op jit(solution)/shard_map/ppermute | solution.py:17
  21.2 40.7 %collective-permute-start.1 = (bf16[256,512]{1,0:T(8,128)(2,1)S(1)}, bf16[256,512]{1,0:T(8,128)(2,1)S(1)}, u32[]{:S(2)}, u32[]{:S(2)}) collective-permute-start(bf16[256,512]{1,0:T(8,128)(2,1)S(1)} %copy-done.8), channel_id=1, source_target_pairs={{0,4},{4,0},{8,12},{12,8},{16,20},{20,16},{24,28},{28,24},{1,5},{5... | collective-permute-start | bytes 786440 | tf_op jit(solution)/shard_map/ppermute | solution.py:17
  22.7 40.6 %collective-permute-start.6 = (bf16[256,512]{1,0:T(8,128)(2,1)S(1)}, bf16[256,512]{1,0:T(8,128)(2,1)S(1)}, u32[]{:S(2)}, u32[]{:S(2)}) collective-permute-start(bf16[256,512]{1,0:T(8,128)(2,1)S(1)} %copy-done.8), channel_id=1, source_target_pairs={{0,24},{4,28},{8,16},{12,20},{16,8},{20,12},{24,0},{28,4},{1,25},{... | collective-permute-start | bytes 786440 | tf_op jit(solution)/shard_map/ppermute | solution.py:17
  40.7 23.6 %collective-permute-start.3 = (bf16[256,512]{1,0:T(8,128)(2,1)S(1)}, bf16[256,512]{1,0:T(8,128)(2,1)S(1)}, u32[]{:S(2)}, u32[]{:S(2)}) collective-permute-start(bf16[256,512]{1,0:T(8,128)(2,1)S(1)} %collective-permute-done.2), channel_id=1, source_target_pairs={{0,4},{4,0},{8,12},{12,8},{16,20},{20,16},{24,28},{28,24},{1,5},{5... | collective-permute-start | bytes 786440 | tf_op jit(solution)/shard_map/ppermute | solution.py:17
  60.8 17.8 %collective-permute-start.5 = (bf16[256,512]{1,0:T(8,128)(2,1)S(1)}, bf16[256,512]{1,0:T(8,128)(2,1)S(1)}, u32[]{:S(2)}, u32[]{:S(2)}) collective-permute-start(bf16[256,512]{1,0:T(8,128)(2,1)S(1)} %collective-permute-done.4), channel_id=1, source_target_pairs={{0,4},{4,0},{8,12},{12,8},{16,20},{20,16},{24,28},{28,24},{1,5},{5... | collective-permute-start | bytes 786440 | tf_op jit(solution)/shard_map/ppermute | solution.py:17
  63.3 16.8 %collective-permute-start.7 = (bf16[256,512]{1,0:T(8,128)(2,1)S(1)}, bf16[256,512]{1,0:T(8,128)(2,1)S(1)}, u32[]{:S(2)}, u32[]{:S(2)}) collective-permute-start(bf16[256,512]{1,0:T(8,128)(2,1)S(1)} %collective-permute-done.6), channel_id=1, source_target_pairs={{0,4},{4,0},{8,12},{12,8},{16,20},{20,16},{24,28},{28,24},{1,5},{5... | collective-permute-start | bytes 786440 | tf_op jit(solution)/shard_map/ppermute | solution.py:17
  65.7 1.0 copy-start
  66.7 14.1 %copy-start.11 = (s32[1,128,2]{1,2,0:T(2,128)S(1)}, s32[1,128,2]{1,2,0:T(2,128)}, u32[]{:S(2)}) copy-start(s32[1,128,2]{1,2,0:T(2,128)} %param.24) | copy-start | bytes 3076
  74.6 18.4 %all-to-all-start.1 = ((bf16[8,128,256]{2,1,0:T(8,128)(2,1)}), bf16[8,128,256]{2,1,0:T(8,128)(2,1)S(1)}, u32[]{:S(2)}, u32[]{:S(2)}) async-start(bf16[8,128,256]{2,1,0:T(8,128)(2,1)} %bitcast.86), calls=%async_computation.1 | async-start | bytes 1048576 | tf_op jit(solution)/shard_map/all_to_all | solution.py:236
  80.8 17.2 %collective-permute-start.8 = (bf16[2048,512]{1,0:T(8,128)(2,1)}, bf16[2048,512]{1,0:T(8,128)(2,1)}, u32[]{:S(2)}, u32[]{:S(2)}) collective-permute-start(bf16[2048,512]{1,0:T(8,128)(2,1)} %constant_dynamic-update-slice_fusion), channel_id=1, source_target_pairs={{0,1},{1,0},{2,3},{3,2},{4,5},{5,4},{6,7},{7,6},{8,9},{9,8},{10,11... | collective-permute-start | bytes 6291464 | tf_op jit(solution)/shard_map/ppermute | solution.py:17
  93.1 12.4 %collective-permute-start = (bf16[128,2048]{1,0:T(8,128)(2,1)S(1)}, bf16[128,2048]{1,0:T(8,128)(2,1)S(1)}, u32[]{:S(2)}, u32[]{:S(2)}) collective-permute-start(bf16[128,2048]{1,0:T(8,128)(2,1)S(1)} %bitcast_dynamic-update-slice_fusion), channel_id=1, source_target_pairs={{0,2},{1,3},{2,0},{3,1},{4,6},{5,7},{6,4},{7,5},{8,10},{9,11},{10,... | collective-permute-start | bytes 1572872 | tf_op jit(solution)/shard_map/ppermute | solution.py:17
  94.8 29.9 %collective-permute-start.17 = (s32[128,2]{1,0:T(8,128)S(1)}, s32[128,2]{1,0:T(8,128)S(1)}, u32[]{:S(2)}, u32[]{:S(2)}) collective-permute-start(s32[128,2]{1,0:T(8,128)S(1)} %broadcast_add_fusion), channel_id=1, source_target_pairs={{0,16},{4,20},{8,24},{12,28},{16,0},{20,4},{24,8},{28,12},{1,17},{... | collective-permute-start | bytes 3080 | tf_op jit(solution)/shard_map/ppermute | solution.py:17
  95.1 29.8 %collective-permute-start.16 = (s32[128,2]{0,1:T(2,128)S(1)}, s32[128,2]{0,1:T(2,128)S(1)}, u32[]{:S(2)}, u32[]{:S(2)}) collective-permute-start(s32[128,2]{0,1:T(2,128)S(1)} %bitcast.91), channel_id=1, source_target_pairs={{0,16},{4,20},{8,24},{12,28},{16,0},{20,4},{24,8},{28,12},{1,17},{... | collective-permute-start | bytes 3080 | tf_op jit(solution)/shard_map/ppermute | solution.py:17
  107.8 4.0 %copy-start.12 = (f32[1,128,2]{1,2,0:T(2,128)S(1)}, f32[1,128,2]{1,2,0:T(2,128)}, u32[]{:S(2)}) copy-start(f32[1,128,2]{1,2,0:T(2,128)} %param.25) | copy-start | bytes 3076
  110.2 6.6 %copy-start.1 = (bf16[1,128,2048]{2,1,0:T(8,128)(2,1)S(1)}, bf16[1,128,2048]{2,1,0:T(8,128)(2,1)}, u32[]{:S(2)}) copy-start(bf16[1,128,2048]{2,1,0:T(8,128)(2,1)} %param.19) | copy-start | bytes 1572868
  110.2 6.9 %copy-start.10 = (f32[2048]{0:T(1024)S(1)}, f32[2048]{0:T(1024)}, u32[]{:S(2)}) copy-start(f32[2048]{0:T(1024)} %param.20) | copy-start | bytes 24580
  110.2 6.4 %collective-permute-start.9 = (bf16[128,1024]{1,0:T(8,128)(2,1)S(1)}, bf16[128,1024]{1,0:T(8,128)(2,1)S(1)}, u32[]{:S(2)}, u32[]{:S(2)}) collective-permute-start(bf16[128,1024]{1,0:T(8,128)(2,1)S(1)} %pad_maximum_fusion.4), channel_id=1, source_target_pairs={{0,2},{1,3},{2,0},{3,1},{4,6},{5,7},{6,4},{7,5},{8,10},{9,11},{10,... | collective-permute-start | bytes 786440 | tf_op jit(solution)/shard_map/ppermute | solution.py:17
  117.3 45.1 %collective-permute-start.18 = (bf16[128,2048]{1,0:T(8,128)(2,1)S(1)}, bf16[128,2048]{1,0:T(8,128)(2,1)S(1)}, u32[]{:S(2)}, u32[]{:S(2)}) collective-permute-start(bf16[128,2048]{1,0:T(8,128)(2,1)S(1)} %multiply_convert_fusion), channel_id=1, source_target_pairs={{0,16},{4,20},{8,24},{12,28},{16,0},{20,4},{24,8},{28,12},{1,17},{... | collective-permute-start | bytes 1572872 | tf_op jit(solution)/shard_map/ppermute | solution.py:17
  121.1 8.5 %collective-permute-start.10 = (bf16[64,2048]{1,0:T(8,128)(2,1)S(1)}, bf16[64,2048]{1,0:T(8,128)(2,1)S(1)}, u32[]{:S(2)}, u32[]{:S(2)}) collective-permute-start(bf16[64,2048]{1,0:T(8,128)(2,1)S(1)} %get-tuple-element.31), channel_id=1, source_target_pairs={{0,4},{4,0},{8,12},{12,8},{16,20},{20,16},{24,28},{28,24},{1,5},{5... | collective-permute-start | bytes 786440 | tf_op jit(solution)/shard_map/ppermute | solution.py:17
  121.1 21.1 %collective-permute-start.11 = (bf16[64,2048]{1,0:T(8,128)(2,1)S(1)}, bf16[64,2048]{1,0:T(8,128)(2,1)S(1)}, u32[]{:S(2)}, u32[]{:S(2)}) collective-permute-start(bf16[64,2048]{1,0:T(8,128)(2,1)S(1)} %get-tuple-element.30), channel_id=1, source_target_pairs={{0,8},{4,12},{8,0},{12,4},{16,24},{20,28},{24,16},{28,20},{1,9},{5... | collective-permute-start | bytes 786440 | tf_op jit(solution)/shard_map/ppermute | solution.py:17
  124.7 19.3 %collective-permute-start.12 = (bf16[64,2048]{1,0:T(8,128)(2,1)S(1)}, bf16[64,2048]{1,0:T(8,128)(2,1)S(1)}, u32[]{:S(2)}, u32[]{:S(2)}) collective-permute-start(bf16[64,2048]{1,0:T(8,128)(2,1)S(1)} %get-tuple-element.29), channel_id=1, source_target_pairs={{0,12},{4,8},{8,4},{12,0},{16,28},{20,24},{24,20},{28,16},{1,13},{... | collective-permute-start | bytes 786440 | tf_op jit(solution)/shard_map/ppermute | solution.py:17
  124.9 42.4 %collective-permute-start.25 = (f32[128,2]{0,1:T(2,128)S(1)}, f32[128,2]{0,1:T(2,128)S(1)}, u32[]{:S(2)}, u32[]{:S(2)}) collective-permute-start(f32[128,2]{0,1:T(2,128)S(1)} %bitcast.94), channel_id=1, source_target_pairs={{0,16},{4,20},{8,24},{12,28},{16,0},{20,4},{24,8},{28,12},{1,17},{... | collective-permute-start | bytes 3080 | tf_op jit(solution)/shard_map/ppermute | solution.py:17
  129.6 14.4 %copy-start.2 = (bf16[64,2048]{1,0:T(8,128)(2,1)}, bf16[64,2048]{1,0:T(8,128)(2,1)S(1)}, u32[]{:S(2)}) copy-start(bf16[64,2048]{1,0:T(8,128)(2,1)S(1)} %collective-permute-done.10.refs_1_) | copy-start | bytes 786436
  142.2 1.7 copy-start.4
  143.9 0.7 copy-start.7
  159.3 8.1 %copy-start.9 = (bf16[64,2048]{1,0:T(8,128)(2,1)S(1)}, bf16[64,2048]{1,0:T(8,128)(2,1)}, u32[]{:S(2)}) copy-start(bf16[64,2048]{1,0:T(8,128)(2,1)} %get-tuple-element.13) | copy-start | bytes 786436
  159.3 37.1 %collective-permute-start.13 = (bf16[64,2048]{1,0:T(8,128)(2,1)}, bf16[64,2048]{1,0:T(8,128)(2,1)}, u32[]{:S(2)}, u32[]{:S(2)}) collective-permute-start(bf16[64,2048]{1,0:T(8,128)(2,1)} %get-tuple-element.14), channel_id=1, source_target_pairs={{0,4},{4,0},{8,12},{12,8},{16,20},{20,16},{24,28},{28,24},{1,5},{5... | collective-permute-start | bytes 786440 | tf_op jit(solution)/shard_map/ppermute | solution.py:17
  163.8 14.4 %collective-permute-start.19 = (bf16[64,2048]{1,0:T(8,128)(2,1)S(1)}, bf16[64,2048]{1,0:T(8,128)(2,1)S(1)}, u32[]{:S(2)}, u32[]{:S(2)}) collective-permute-start(bf16[64,2048]{1,0:T(8,128)(2,1)S(1)} %get-tuple-element.27), channel_id=1, source_target_pairs={{0,4},{4,0},{8,12},{12,8},{16,20},{20,16},{24,28},{28,24},{1,5},{5... | collective-permute-start | bytes 786440 | tf_op jit(solution)/shard_map/ppermute | solution.py:17
  163.8 14.4 %collective-permute-start.20 = (bf16[64,2048]{1,0:T(8,128)(2,1)S(1)}, bf16[64,2048]{1,0:T(8,128)(2,1)S(1)}, u32[]{:S(2)}, u32[]{:S(2)}) collective-permute-start(bf16[64,2048]{1,0:T(8,128)(2,1)S(1)} %get-tuple-element.26), channel_id=1, source_target_pairs={{0,8},{4,12},{8,0},{12,4},{16,24},{20,28},{24,16},{28,20},{1,9},{5... | collective-permute-start | bytes 786440 | tf_op jit(solution)/shard_map/ppermute | solution.py:17
  163.9 16.1 %collective-permute-start.21 = (bf16[64,2048]{1,0:T(8,128)(2,1)S(1)}, bf16[64,2048]{1,0:T(8,128)(2,1)S(1)}, u32[]{:S(2)}, u32[]{:S(2)}) collective-permute-start(bf16[64,2048]{1,0:T(8,128)(2,1)S(1)} %get-tuple-element.25), channel_id=1, source_target_pairs={{0,12},{4,8},{8,4},{12,0},{16,28},{20,24},{24,20},{28,16},{1,13},{... | collective-permute-start | bytes 786440 | tf_op jit(solution)/shard_map/ppermute | solution.py:17
  167.3 44.1 %collective-permute-start.14 = (bf16[64,2048]{1,0:T(8,128)(2,1)}, bf16[64,2048]{1,0:T(8,128)(2,1)S(1)}, u32[]{:S(2)}, u32[]{:S(2)}) collective-permute-start(bf16[64,2048]{1,0:T(8,128)(2,1)} %get-tuple-element.15), channel_id=1, source_target_pairs={{0,8},{4,12},{8,0},{12,4},{16,24},{20,28},{24,16},{28,20},{1,9},{5... | collective-permute-start | bytes 786440 | tf_op jit(solution)/shard_map/ppermute | solution.py:17
  178.2 1.8 copy-start.3
  178.2 33.2 %collective-permute-start.15 = (bf16[64,2048]{1,0:T(8,128)(2,1)}, bf16[64,2048]{1,0:T(8,128)(2,1)S(1)}, u32[]{:S(2)}, u32[]{:S(2)}) collective-permute-start(bf16[64,2048]{1,0:T(8,128)(2,1)} %get-tuple-element.16), channel_id=1, source_target_pairs={{0,12},{4,8},{8,4},{12,0},{16,28},{20,24},{24,20},{28,16},{1,13},{... | collective-permute-start | bytes 786440 | tf_op jit(solution)/shard_map/ppermute | solution.py:17
  178.3 1.8 copy-start.5
  180.1 0.7 copy-start.6
  195.4 7.2 %collective-permute-start.22 = (bf16[64,2048]{1,0:T(8,128)(2,1)}, bf16[64,2048]{1,0:T(8,128)(2,1)S(1)}, u32[]{:S(2)}, u32[]{:S(2)}) collective-permute-start(bf16[64,2048]{1,0:T(8,128)(2,1)} %get-tuple-element.18), channel_id=1, source_target_pairs={{0,4},{4,0},{8,12},{12,8},{16,20},{20,16},{24,28},{28,24},{1,5},{5... | collective-permute-start | bytes 786440 | tf_op jit(solution)/shard_map/ppermute | solution.py:17
  197.3 7.7 %collective-permute-start.23 = (bf16[64,2048]{1,0:T(8,128)(2,1)}, bf16[64,2048]{1,0:T(8,128)(2,1)S(1)}, u32[]{:S(2)}, u32[]{:S(2)}) collective-permute-start(bf16[64,2048]{1,0:T(8,128)(2,1)} %get-tuple-element.19), channel_id=1, source_target_pairs={{0,8},{4,12},{8,0},{12,4},{16,24},{20,28},{24,16},{28,20},{1,9},{5... | collective-permute-start | bytes 786440 | tf_op jit(solution)/shard_map/ppermute | solution.py:17
  199.7 10.9 %collective-permute-start.24 = (bf16[64,2048]{1,0:T(8,128)(2,1)}, bf16[64,2048]{1,0:T(8,128)(2,1)S(1)}, u32[]{:S(2)}, u32[]{:S(2)}) collective-permute-start(bf16[64,2048]{1,0:T(8,128)(2,1)} %get-tuple-element.20), channel_id=1, source_target_pairs={{0,12},{4,8},{8,4},{12,0},{16,28},{20,24},{24,20},{28,16},{1,13},{... | collective-permute-start | bytes 786440 | tf_op jit(solution)/shard_map/ppermute | solution.py:17
  211.4 15.8 %collective-permute-start.26 = (bf16[128,2048]{1,0:T(8,128)(2,1)S(1)}, bf16[128,2048]{1,0:T(8,128)(2,1)S(1)}, u32[]{:S(2)}, u32[]{:S(2)}) collective-permute-start(bf16[128,2048]{1,0:T(8,128)(2,1)S(1)} %fusion.5), channel_id=1, source_target_pairs={{0,16},{4,20},{8,24},{12,28},{16,0},{20,4},{24,8},{28,12},{1,17},{... | collective-permute-start | bytes 1572872 | tf_op jit(solution)/shard_map/ppermute | solution.py:17

commit v2 on v1

--- a/solution.py
+++ b/solution.py
@@ -4,6 +4,7 @@
 from jax.experimental import pallas as pl
 from jax.experimental.pallas import tpu as pltpu
 from jax.sharding import PartitionSpec as P
+
 
 GRID_W = 64
 EPS = 1e-06
@@ -187,7 +188,6 @@
     group = heads // kv_heads
     per = heads // parts
     kv_per = max(1, per // group)
-    model = residual.shape[-1]
     half = parts // 2
     near = parts // 4
 
@@ -201,14 +201,9 @@
     )
     by_head = lax.all_to_all(packed, "sp", split_axis=0, concat_axis=0, tiled=True)
 
-    shards = [None] * parts
+    shards = [None] * 4
     for far in range(4):
-        shard = out_weight if far == 0 else swap(out_weight, "sp", far * near)
-        shards[far * near] = shard
-        for close in range(1, near):
-            shards[far * near + close] = swap(shard, "sp", close)
-    own_columns = jnp.concatenate(shards, axis=0)
-    core_columns = swap(own_columns, "dp", 1)
+        shards[far] = out_weight if far == 0 else swap(out_weight, "sp", far * near)
 
     experts = expert_gate.shape[0] * parts
     capacity = max(2, 4 * (tokens // 2) // experts)
@@ -233,6 +228,14 @@
     pick_far = selection(chosen_far, slot_far)
 
     attended = attend(by_head.reshape(parts * tokens, -1), per, kv_per, width)
+    attended, shards = lax.optimization_barrier((attended, shards))
+    whole = []
+    for far in range(4):
+        whole.append(shards[far])
+        for close in range(1, near):
+            whole.append(swap(shards[far], "sp", close))
+    own_columns = jnp.concatenate(whole, axis=0)
+    core_columns = swap(own_columns, "dp", 1)
     returned = lax.all_to_all(
         attended.reshape(parts, tokens, per * width), "sp", split_axis=0, concat_axis=0, tiled=True
     )
@@ -268,15 +271,21 @@
 
     normed_far = swap(normed, "sp", half)
 
-    def serve(source, picks):
+    def send(source, picks):
         chosen_rows = (picks[0] | picks[1]).astype(BF16)
         sent = lax.dot_general(
             chosen_rows, source, (((0,), (0,)), ((), ())), preferred_element_type=F32
         ).astype(BF16)
-        blocks = [sent[k * slots : (k + 1) * slots] for k in range(half)]
-        blocks = [blocks[0]] + [swap(blocks[k], "sp", k) for k in range(1, half)]
-        results = expert_rows(blocks, expert_gate[0], expert_up[0], expert_down[0])
-        return [results[0]] + [swap(results[k], "sp", k) for k in range(1, half)]
+        return exchange([sent[k * slots : (k + 1) * slots] for k in range(half)])
+
+    def exchange(blocks):
+        moved = [blocks[0]]
+        for k in range(1, half):
+            moved.append(swap(blocks[k], "sp", k))
+        return moved
+
+    def serve(blocks):
+        return expert_rows(blocks, expert_gate[0], expert_up[0], expert_down[0])
 
     def combine(results, picks, weight):
         flat = jnp.concatenate(results, axis=0)
@@ -285,8 +294,12 @@
             for j in range(2)
         )
 
-    near_results = serve(normed, pick)
-    far_results = serve(normed_far, pick_far)
+    near_blocks = send(normed, pick)
+    far_blocks = send(normed_far, pick_far)
+    near_results = serve(near_blocks)
+    far_results = serve(far_blocks)
+    near_results = exchange(near_results)
+    far_results = exchange(far_results)
     crossed = swap(combine(far_results, pick_far, weight_far).astype(BF16), "sp", half)
     result = mixed_sum + combine(near_results, pick, weight) + crossed.astype(F32)
     return result.astype(BF16)[None]
@@ -309,6 +322,7 @@
         P("dp", "sp", None),
     )
     out_specs = P("dp", "sp", None)
+
     return jax.shard_map(
         on_device, mesh=mesh, in_specs=in_specs, out_specs=out_specs, check_vma=False
     )

time: 229 us -> 233 us (1.017)
  starting transfers between devices: 45.2 us -> 50.4 us
    all_to_all x1, waiting for transfers between devices: 0.01 us -> 33.9 us  [on_device(): lax.all_to_all(packed, 'sp', split_axis=0, concat_axis=0, tiled=True)]
    ppermute x27, waiting for transfers between devices: 103 us -> 80.4 us  [swap(): return lax.ppermute(array, axis, [(i, i ^ bits) for i in range(size)])]
    all_to_all x1, waiting for transfers between devices: 11.4 us -> 0.01 us  [on_device(): lax.all_to_all(attended.reshape(parts, tokens, per * width), 'sp', split_...]
    ppermute x27, starting transfers between devices: 33.9 us -> 39.5 us  [swap(): return lax.ppermute(array, axis, [(i, i ^ bits) for i in range(size)])]
    unnamed x48 -> x50, local copies, waits for them, and re-layouts: 11.7 us -> 11.7 us
  transfers between devices with their start and end apart: 29 -> 29, of which waited for: 14 -> 16; matrix products, arithmetic and copies ran while one was open for 8% -> 7% of each run, Pallas kernels for 16% -> 16%
where the time goes in v2:
time: 233 us; the launch traced here: 232 us
  waiting for transfers between devices  114 us (49%)
  starting transfers between devices  50.4 us (22%)
  Pallas kernels  41.9 us (18%)
  local copies, waits for them, and re-layouts  16.6 us (7%)
  matrix products  6.74 us (3%)
    ppermute x27, waiting for transfers between devices, swap(): return lax.ppermute(array, axis, [(i, i ^ bits) for i in range(size)])  80.4 us
    ppermute x27, starting transfers between devices, swap(): return lax.ppermute(array, axis, [(i, i ^ bits) for i in range(size)])  39.5 us
    all_to_all x1, waiting for transfers between devices, on_device(): lax.all_to_all(packed, 'sp', split_axis=0, concat_axis=0, tiled=True)  33.9 us
    pallas_call x2, Pallas kernels, expert_rows(): pl.pallas_call(body, grid=(steps,), in_specs=[whole] * count + [pl.BlockS...  29.2 us
    unnamed x50, local copies, waits for them, and re-layouts  11.7 us
    pallas_call x1, Pallas kernels, attend(): pl.pallas_call(body, grid=(length // rows,), in_specs=[pl.BlockSpec((rows...  7.84 us
    all_to_all x1, starting transfers between devices, on_device(): lax.all_to_all(packed, 'sp', split_axis=0, concat_axis=0, tiled=True)  7.29 us
    pallas_call x1, Pallas kernels, pack_rows(): pl.pallas_call(body, out_shape=jax.ShapeDtypeStruct((parts, rows, block),...  4.85 us
  transfers between devices with their start and end apart: 29, of which 16 were waited for; matrix products, arithmetic and copies ran while one was open for 7% of the time, Pallas kernels for 16%

profile of v2, /device:TPU:0, one launch (start us, length us, event | category | flops | bytes accessed | tf_op | source)
XLA Modules:
  0.0 232.1 jit_solution(15382451203774752319)
XLA Ops:
  0.0 2.0 copy.22
  2.0 1.7 copy_bitcast_fusion.1
  3.7 1.0 sine_multiply_fusion
  4.7 4.8 %pack_rows.1 = bf16[8,128,512]{2,1,0:T(8,128)(2,1)} custom-call(bf16[128,2048]{1,0:T(8,128)(2,1)} %bitcast.87, bf16[128,512]{1,0:T(8,128)(2,1)} %get-tuple-element.64.k_ref, bf16[128,512]{1,0:T(8,128)(2,1)} %get-tuple-element.63.v_ref, f32[1,128]{1,0:T(1,128)} %bitcast.95, f32[1,128]{1,0:T(1,128)} %bitcast.96, f32[128,128]{1,0:T(8,128)} %get-tuple-element.48.c_ref, ...), custom_call_target="tpu_custom_call" | custom-call | tf_op jit(solution)/shard_map/pack_rows/pallas_call | solution.py:74
  9.6 7.3 %all-to-all-start = ((bf16[8,128,512]{2,1,0:T(8,128)(2,1)}), bf16[8,128,512]{2,1,0:T(8,128)(2,1)S(1)}, u32[]{:S(2)}, u32[]{:S(2)}) async-start(bf16[8,128,512]{2,1,0:T(8,128)(2,1)} %pack_rows.1), calls=%async_computation | async-start | bytes 2097152 | tf_op jit(solution)/shard_map/all_to_all | solution.py:202
  16.8 2.0 collective-permute-start
  18.9 2.4 %collective-permute-start.1 = (bf16[256,512]{1,0:T(8,128)(2,1)S(1)}, bf16[256,512]{1,0:T(8,128)(2,1)S(1)}, u32[]{:S(2)}, u32[]{:S(2)}) collective-permute-start(bf16[256,512]{1,0:T(8,128)(2,1)S(1)} %copy-done.8), channel_id=1, source_target_pairs={{0,16},{4,20},{8,24},{12,28},{16,0},{20,4},{24,8},{28,12},{1,17},{... | collective-permute-start | bytes 786440 | tf_op jit(solution)/shard_map/ppermute | solution.py:18
  21.3 33.9 %all-to-all-done = bf16[8,128,512]{2,1,0:T(8,128)(2,1)S(1)} async-done(((bf16[8,128,512]{2,1,0:T(8,128)(2,1)}), bf16[8,128,512]{2,1,0:T(8,128)(2,1)S(1)}, u32[]{:S(2)}, u32[]{:S(2)}) %all-to-all-start) | async-done | bytes 1048608 | tf_op jit(solution)/shard_map/all_to_all | solution.py:202
  55.2 1.0 copy-done
  56.2 7.8 %attend.1 = bf16[1024,256]{1,0:T(8,128)(2,1)} custom-call(bf16[1024,512]{1,0:T(8,128)(2,1)} %bitcast.84, bf16[1024,512]{1,0:T(8,128)(2,1)} %bitcast.85), custom_call_target="tpu_custom_call" | custom-call | tf_op jit(solution)/shard_map/attend/pallas_call | solution.py:98
  64.1 2.0 collective-permute-start.5
  66.9 1.9 collective-permute-start.7
  68.9 3.7 %all-to-all-start.1 = ((bf16[8,128,256]{2,1,0:T(8,128)(2,1)}), bf16[8,128,256]{2,1,0:T(8,128)(2,1)S(1)}, u32[]{:S(2)}, u32[]{:S(2)}) async-start(bf16[8,128,256]{2,1,0:T(8,128)(2,1)} %bitcast.86), calls=%async_computation.1 | async-start | bytes 1048576 | tf_op jit(solution)/shard_map/all_to_all | solution.py:239
  74.0 0.7 constant_dynamic-update-slice_fusion.5
  74.8 7.1 %collective-permute-done.5 = bf16[256,512]{1,0:T(8,128)(2,1)S(1)} collective-permute-done((bf16[256,512]{1,0:T(8,128)(2,1)S(1)}, bf16[256,512]{1,0:T(8,128)(2,1)S(1)}, u32[]{:S(2)}, u32[]{:S(2)}) %collective-permute-start.5) | collective-permute-done | bytes 262176 | tf_op jit(solution)/shard_map/ppermute | solution.py:18
  83.3 2.1 collective-permute-done.6
  85.4 0.8 constant_dynamic-update-slice_fusion.2
  86.9 1.4 collective-permute-done.7
  89.9 1.6 collective-permute-start.3
  91.5 7.2 %collective-permute-start.17 = (s32[128,2]{1,0:T(8,128)S(1)}, s32[128,2]{1,0:T(8,128)S(1)}, u32[]{:S(2)}, u32[]{:S(2)}) collective-permute-start(s32[128,2]{1,0:T(8,128)S(1)} %broadcast_add_fusion), channel_id=1, source_target_pairs={{0,16},{4,20},{8,24},{12,28},{16,0},{20,4},{24,8},{28,12},{1,17},{... | collective-permute-start | bytes 3080 | tf_op jit(solution)/shard_map/ppermute | solution.py:18
  99.0 5.3 %collective-permute-done.3 = bf16[128,2048]{1,0:T(8,128)(2,1)S(1)} collective-permute-done((bf16[128,2048]{1,0:T(8,128)(2,1)S(1)}, bf16[128,2048]{1,0:T(8,128)(2,1)S(1)}, u32[]{:S(2)}, u32[]{:S(2)}) %collective-permute-start.3) | collective-permute-done | bytes 524320 | tf_op jit(solution)/shard_map/ppermute | solution.py:18
  104.3 2.3 convolution_convert_fusion.2
  106.6 0.7 broadcast_select_fusion.1
  107.4 1.6 collective-permute-start.9
  109.0 6.3 %collective-permute-done.9 = bf16[128,1024]{1,0:T(8,128)(2,1)S(1)} collective-permute-done((bf16[128,1024]{1,0:T(8,128)(2,1)S(1)}, bf16[128,1024]{1,0:T(8,128)(2,1)S(1)}, u32[]{:S(2)}, u32[]{:S(2)}) %collective-permute-start.9) | collective-permute-done | bytes 262176 | tf_op jit(solution)/shard_map/ppermute | solution.py:18
  115.9 7.2 %collective-permute-start.18 = (bf16[128,2048]{1,0:T(8,128)(2,1)S(1)}, bf16[128,2048]{1,0:T(8,128)(2,1)S(1)}, u32[]{:S(2)}, u32[]{:S(2)}) collective-permute-start(bf16[128,2048]{1,0:T(8,128)(2,1)S(1)} %multiply_convert_fusion), channel_id=1, source_target_pairs={{0,16},{4,20},{8,24},{12,28},{16,0},{20,4},{24,8},{28,12},{1,17},{... | collective-permute-start | bytes 1572872 | tf_op jit(solution)/shard_map/ppermute | solution.py:18
  123.7 0.8 fusion.54
  124.5 1.7 collective-permute-start.10
  126.2 1.8 collective-permute-start.12
  128.5 4.3 %collective-permute-done.10.refs_1_ = bf16[64,2048]{1,0:T(8,128)(2,1)S(1)} collective-permute-done((bf16[64,2048]{1,0:T(8,128)(2,1)S(1)}, bf16[64,2048]{1,0:T(8,128)(2,1)S(1)}, u32[]{:S(2)}, u32[]{:S(2)}) %collective-permute-start.10) | collective-permute-done | bytes 262176 | tf_op jit(solution)/shard_map/ppermute | solution.py:18
  132.8 12.6 %collective-permute-done.11.refs_2_ = bf16[64,2048]{1,0:T(8,128)(2,1)S(1)} collective-permute-done((bf16[64,2048]{1,0:T(8,128)(2,1)S(1)}, bf16[64,2048]{1,0:T(8,128)(2,1)S(1)}, u32[]{:S(2)}, u32[]{:S(2)}) %collective-permute-start.11) | collective-permute-done | bytes 262176 | tf_op jit(solution)/shard_map/ppermute | solution.py:18
  145.4 2.6 %collective-permute-done.12.refs_3_ = bf16[64,2048]{1,0:T(8,128)(2,1)S(1)} collective-permute-done((bf16[64,2048]{1,0:T(8,128)(2,1)S(1)}, bf16[64,2048]{1,0:T(8,128)(2,1)S(1)}, u32[]{:S(2)}, u32[]{:S(2)}) %collective-permute-start.12) | collective-permute-done | bytes 262176 | tf_op jit(solution)/shard_map/ppermute | solution.py:18
  148.7 14.6 %expert_rows.2 = (bf16[64,2048]{1,0:T(8,128)(2,1)}, bf16[64,2048]{1,0:T(8,128)(2,1)}, bf16[64,2048]{1,0:T(8,128)(2,1)}, bf16[64,2048]{1,0:T(8,128)(2,1)}) custom-call(bf16[64,2048]{1,0:T(8,128)(2,1)} %get-tuple-element.42.refs_0_, bf16[64,2048]{1,0:T(8,128)(2,1)} %copy-done.2, bf16[64,2048]{1,0:T(8,128)(2,1)} %copy-done.4, bf16[64,2048]{1,0:T(8,128)(2,1)} %copy-done.7, ...), custom_call_target="tpu_custom_call" | custom-call | tf_op jit(solution)/shard_map/expert_rows/pallas_call | solution.py:150
  163.3 1.7 collective-permute-start.13
  165.7 0.8 fusion.53
  166.9 3.0 %collective-permute-start.21 = (bf16[64,2048]{1,0:T(8,128)(2,1)S(1)}, bf16[64,2048]{1,0:T(8,128)(2,1)S(1)}, u32[]{:S(2)}, u32[]{:S(2)}) collective-permute-start(bf16[64,2048]{1,0:T(8,128)(2,1)S(1)} %get-tuple-element.35), channel_id=1, source_target_pairs={{0,12},{4,8},{8,4},{12,0},{16,28},{20,24},{24,20},{28,16},{1,13},{... | collective-permute-start | bytes 786440 | tf_op jit(solution)/shard_map/ppermute | solution.py:18
  170.0 11.1 %collective-permute-done.19.refs_1_ = bf16[64,2048]{1,0:T(8,128)(2,1)S(1)} collective-permute-done((bf16[64,2048]{1,0:T(8,128)(2,1)S(1)}, bf16[64,2048]{1,0:T(8,128)(2,1)S(1)}, u32[]{:S(2)}, u32[]{:S(2)}) %collective-permute-start.19) | collective-permute-done | bytes 262176 | tf_op jit(solution)/shard_map/ppermute | solution.py:18
  181.1 1.6 collective-permute-done.21.refs_3_
  183.4 14.6 %expert_rows.3 = (bf16[64,2048]{1,0:T(8,128)(2,1)}, bf16[64,2048]{1,0:T(8,128)(2,1)}, bf16[64,2048]{1,0:T(8,128)(2,1)}, bf16[64,2048]{1,0:T(8,128)(2,1)}) custom-call(bf16[64,2048]{1,0:T(8,128)(2,1)} %get-tuple-element.38.refs_0_, bf16[64,2048]{1,0:T(8,128)(2,1)} %copy-done.3, bf16[64,2048]{1,0:T(8,128)(2,1)} %copy-done.5, bf16[64,2048]{1,0:T(8,128)(2,1)} %copy-done.6, ...), custom_call_target="tpu_custom_call" | custom-call | tf_op jit(solution)/shard_map/expert_rows/pallas_call | solution.py:150
  198.0 1.2 collective-permute-start.22
  199.2 1.0 constant_dynamic-update-slice_fusion.10
  200.2 1.5 collective-permute-start.23
  201.7 1.0 constant_dynamic-update-slice_fusion.15
  202.6 1.5 collective-permute-start.24
  204.6 4.5 %collective-permute-done.23 = bf16[64,2048]{1,0:T(8,128)(2,1)S(1)} collective-permute-done((bf16[64,2048]{1,0:T(8,128)(2,1)}, bf16[64,2048]{1,0:T(8,128)(2,1)S(1)}, u32[]{:S(2)}, u32[]{:S(2)}) %collective-permute-start.23) | collective-permute-done | bytes 262176 | tf_op jit(solution)/shard_map/ppermute | solution.py:18
  209.2 5.1 %collective-permute-done.24 = bf16[64,2048]{1,0:T(8,128)(2,1)S(1)} collective-permute-done((bf16[64,2048]{1,0:T(8,128)(2,1)}, bf16[64,2048]{1,0:T(8,128)(2,1)S(1)}, u32[]{:S(2)}, u32[]{:S(2)}) %collective-permute-start.24) | collective-permute-done | bytes 262176 | tf_op jit(solution)/shard_map/ppermute | solution.py:18
  215.5 15.2 %collective-permute-done.26 = bf16[128,2048]{1,0:T(8,128)(2,1)S(1)} collective-permute-done((bf16[128,2048]{1,0:T(8,128)(2,1)S(1)}, bf16[128,2048]{1,0:T(8,128)(2,1)S(1)}, u32[]{:S(2)}, u32[]{:S(2)}) %collective-permute-start.26) | collective-permute-done | bytes 524320 | tf_op jit(solution)/shard_map/ppermute | solution.py:18
  230.8 1.3 fusion.6
  (103 shorter events, 12.3 us)
Async XLA Ops:
  3.7 13.1 %copy-start.8 = (bf16[256,512]{1,0:T(8,128)(2,1)S(1)}, bf16[256,512]{1,0:T(8,128)(2,1)}, u32[]{:S(2)}) copy-start(bf16[256,512]{1,0:T(8,128)(2,1)} %param.18) | copy-start | bytes 786436
  9.6 45.7 %all-to-all-start = ((bf16[8,128,512]{2,1,0:T(8,128)(2,1)}), bf16[8,128,512]{2,1,0:T(8,128)(2,1)S(1)}, u32[]{:S(2)}, u32[]{:S(2)}) async-start(bf16[8,128,512]{2,1,0:T(8,128)(2,1)} %pack_rows.1), calls=%async_computation | async-start | bytes 2097152 | tf_op jit(solution)/shard_map/all_to_all | solution.py:202
  16.8 47.2 %collective-permute-start = (bf16[256,512]{1,0:T(8,128)(2,1)S(1)}, bf16[256,512]{1,0:T(8,128)(2,1)S(1)}, u32[]{:S(2)}, u32[]{:S(2)}) collective-permute-start(bf16[256,512]{1,0:T(8,128)(2,1)S(1)} %copy-done.8), channel_id=1, source_target_pairs={{0,8},{4,12},{8,0},{12,4},{16,24},{20,28},{24,16},{28,20},{1,9},{5... | collective-permute-start | bytes 786440 | tf_op jit(solution)/shard_map/ppermute | solution.py:18
  18.9 45.2 %collective-permute-start.1 = (bf16[256,512]{1,0:T(8,128)(2,1)S(1)}, bf16[256,512]{1,0:T(8,128)(2,1)S(1)}, u32[]{:S(2)}, u32[]{:S(2)}) collective-permute-start(bf16[256,512]{1,0:T(8,128)(2,1)S(1)} %copy-done.8), channel_id=1, source_target_pairs={{0,16},{4,20},{8,24},{12,28},{16,0},{20,4},{24,8},{28,12},{1,17},{... | collective-permute-start | bytes 786440 | tf_op jit(solution)/shard_map/ppermute | solution.py:18
  21.2 42.8 %collective-permute-start.2 = (bf16[256,512]{1,0:T(8,128)(2,1)S(1)}, bf16[256,512]{1,0:T(8,128)(2,1)S(1)}, u32[]{:S(2)}, u32[]{:S(2)}) collective-permute-start(bf16[256,512]{1,0:T(8,128)(2,1)S(1)} %copy-done.8), channel_id=1, source_target_pairs={{0,24},{4,28},{8,16},{12,20},{16,8},{20,12},{24,0},{28,4},{1,25},{... | collective-permute-start | bytes 786440 | tf_op jit(solution)/shard_map/ppermute | solution.py:18
  55.2 1.0 copy-start
  64.1 9.2 %collective-permute-start.4 = (bf16[256,512]{1,0:T(8,128)(2,1)S(1)}, bf16[256,512]{1,0:T(8,128)(2,1)S(1)}, u32[]{:S(2)}, u32[]{:S(2)}) collective-permute-start(bf16[256,512]{1,0:T(8,128)(2,1)S(1)} %copy-done.8), channel_id=1, source_target_pairs={{0,4},{4,0},{8,12},{12,8},{16,20},{20,16},{24,28},{28,24},{1,5},{5... | collective-permute-start | bytes 786440 | tf_op jit(solution)/shard_map/ppermute | solution.py:18
  64.1 17.8 %collective-permute-start.5 = (bf16[256,512]{1,0:T(8,128)(2,1)S(1)}, bf16[256,512]{1,0:T(8,128)(2,1)S(1)}, u32[]{:S(2)}, u32[]{:S(2)}) collective-permute-start(bf16[256,512]{1,0:T(8,128)(2,1)S(1)} %collective-permute-done), channel_id=1, source_target_pairs={{0,4},{4,0},{8,12},{12,8},{16,20},{20,16},{24,28},{28,24},{1,5},{5... | collective-permute-start | bytes 786440 | tf_op jit(solution)/shard_map/ppermute | solution.py:18
  66.9 18.6 %collective-permute-start.6 = (bf16[256,512]{1,0:T(8,128)(2,1)S(1)}, bf16[256,512]{1,0:T(8,128)(2,1)S(1)}, u32[]{:S(2)}, u32[]{:S(2)}) collective-permute-start(bf16[256,512]{1,0:T(8,128)(2,1)S(1)} %collective-permute-done.1), channel_id=1, source_target_pairs={{0,4},{4,0},{8,12},{12,8},{16,20},{20,16},{24,28},{28,24},{1,5},{5... | collective-permute-start | bytes 786440 | tf_op jit(solution)/shard_map/ppermute | solution.py:18
  66.9 21.3 %collective-permute-start.7 = (bf16[256,512]{1,0:T(8,128)(2,1)S(1)}, bf16[256,512]{1,0:T(8,128)(2,1)S(1)}, u32[]{:S(2)}, u32[]{:S(2)}) collective-permute-start(bf16[256,512]{1,0:T(8,128)(2,1)S(1)} %collective-permute-done.2), channel_id=1, source_target_pairs={{0,4},{4,0},{8,12},{12,8},{16,20},{20,16},{24,28},{28,24},{1,5},{5... | collective-permute-start | bytes 786440 | tf_op jit(solution)/shard_map/ppermute | solution.py:18
  68.9 20.8 %all-to-all-start.1 = ((bf16[8,128,256]{2,1,0:T(8,128)(2,1)}), bf16[8,128,256]{2,1,0:T(8,128)(2,1)S(1)}, u32[]{:S(2)}, u32[]{:S(2)}) async-start(bf16[8,128,256]{2,1,0:T(8,128)(2,1)} %bitcast.86), calls=%async_computation.1 | async-start | bytes 1048576 | tf_op jit(solution)/shard_map/all_to_all | solution.py:239
  72.6 16.4 %copy-start.12 = (s32[1,128,2]{1,2,0:T(2,128)S(1)}, s32[1,128,2]{1,2,0:T(2,128)}, u32[]{:S(2)}) copy-start(s32[1,128,2]{1,2,0:T(2,128)} %param.24) | copy-start | bytes 3076
  89.0 15.3 %collective-permute-start.8 = (bf16[2048,512]{1,0:T(8,128)(2,1)}, bf16[2048,512]{1,0:T(8,128)(2,1)}, u32[]{:S(2)}, u32[]{:S(2)}) collective-permute-start(bf16[2048,512]{1,0:T(8,128)(2,1)} %constant_dynamic-update-slice_fusion), channel_id=1, source_target_pairs={{0,1},{1,0},{2,3},{3,2},{4,5},{5,4},{6,7},{7,6},{8,9},{9,8},{10,11... | collective-permute-start | bytes 6291464 | tf_op jit(solution)/shard_map/ppermute | solution.py:18
  89.9 14.4 %collective-permute-start.3 = (bf16[128,2048]{1,0:T(8,128)(2,1)S(1)}, bf16[128,2048]{1,0:T(8,128)(2,1)S(1)}, u32[]{:S(2)}, u32[]{:S(2)}) collective-permute-start(bf16[128,2048]{1,0:T(8,128)(2,1)S(1)} %bitcast_dynamic-update-slice_fusion), channel_id=1, source_target_pairs={{0,2},{1,3},{2,0},{3,1},{4,6},{5,7},{6,4},{7,5},{8,10},{9,11},{10,... | collective-permute-start | bytes 1572872 | tf_op jit(solution)/shard_map/ppermute | solution.py:18
  91.5 34.7 %collective-permute-start.17 = (s32[128,2]{1,0:T(8,128)S(1)}, s32[128,2]{1,0:T(8,128)S(1)}, u32[]{:S(2)}, u32[]{:S(2)}) collective-permute-start(s32[128,2]{1,0:T(8,128)S(1)} %broadcast_add_fusion), channel_id=1, source_target_pairs={{0,16},{4,20},{8,24},{12,28},{16,0},{20,4},{24,8},{28,12},{1,17},{... | collective-permute-start | bytes 3080 | tf_op jit(solution)/shard_map/ppermute | solution.py:18
  98.7 29.5 %collective-permute-start.16 = (s32[128,2]{0,1:T(2,128)S(1)}, s32[128,2]{0,1:T(2,128)S(1)}, u32[]{:S(2)}, u32[]{:S(2)}) collective-permute-start(s32[128,2]{0,1:T(2,128)S(1)} %bitcast.91), channel_id=1, source_target_pairs={{0,16},{4,20},{8,24},{12,28},{16,0},{20,4},{24,8},{28,12},{1,17},{... | collective-permute-start | bytes 3080 | tf_op jit(solution)/shard_map/ppermute | solution.py:18
  99.0 7.6 %copy-start.10 = (bf16[2048,512]{1,0:T(8,128)(2,1)S(1)}, bf16[2048,512]{1,0:T(8,128)(2,1)}, u32[]{:S(2)}) copy-start(bf16[2048,512]{1,0:T(8,128)(2,1)} %constant_dynamic-update-slice_fusion) | copy-start | bytes 6291460
  106.6 2.4 %copy-start.13 = (f32[1,128,2]{1,2,0:T(2,128)S(1)}, f32[1,128,2]{1,2,0:T(2,128)}, u32[]{:S(2)}) copy-start(f32[1,128,2]{1,2,0:T(2,128)} %param.25) | copy-start | bytes 3076
  107.3 8.1 %copy-start.1 = (bf16[1,128,2048]{2,1,0:T(8,128)(2,1)S(1)}, bf16[1,128,2048]{2,1,0:T(8,128)(2,1)}, u32[]{:S(2)}) copy-start(bf16[1,128,2048]{2,1,0:T(8,128)(2,1)} %param.19) | copy-start | bytes 1572868
  107.3 8.4 %copy-start.11 = (f32[2048]{0:T(1024)S(1)}, f32[2048]{0:T(1024)}, u32[]{:S(2)}) copy-start(f32[2048]{0:T(1024)} %param.20) | copy-start | bytes 24580
  107.4 7.9 %collective-permute-start.9 = (bf16[128,1024]{1,0:T(8,128)(2,1)S(1)}, bf16[128,1024]{1,0:T(8,128)(2,1)S(1)}, u32[]{:S(2)}, u32[]{:S(2)}) collective-permute-start(bf16[128,1024]{1,0:T(8,128)(2,1)S(1)} %pad_maximum_fusion.4), channel_id=1, source_target_pairs={{0,2},{1,3},{2,0},{3,1},{4,6},{5,7},{6,4},{7,5},{8,10},{9,11},{10,... | collective-permute-start | bytes 786440 | tf_op jit(solution)/shard_map/ppermute | solution.py:18
  115.9 49.1 %collective-permute-start.18 = (bf16[128,2048]{1,0:T(8,128)(2,1)S(1)}, bf16[128,2048]{1,0:T(8,128)(2,1)S(1)}, u32[]{:S(2)}, u32[]{:S(2)}) collective-permute-start(bf16[128,2048]{1,0:T(8,128)(2,1)S(1)} %multiply_convert_fusion), channel_id=1, source_target_pairs={{0,16},{4,20},{8,24},{12,28},{16,0},{20,4},{24,8},{28,12},{1,17},{... | collective-permute-start | bytes 1572872 | tf_op jit(solution)/shard_map/ppermute | solution.py:18
  124.5 8.3 %collective-permute-start.10 = (bf16[64,2048]{1,0:T(8,128)(2,1)S(1)}, bf16[64,2048]{1,0:T(8,128)(2,1)S(1)}, u32[]{:S(2)}, u32[]{:S(2)}) collective-permute-start(bf16[64,2048]{1,0:T(8,128)(2,1)S(1)} %get-tuple-element.41), channel_id=1, source_target_pairs={{0,4},{4,0},{8,12},{12,8},{16,20},{20,16},{24,28},{28,24},{1,5},{5... | collective-permute-start | bytes 786440 | tf_op jit(solution)/shard_map/ppermute | solution.py:18
  126.2 19.2 %collective-permute-start.11 = (bf16[64,2048]{1,0:T(8,128)(2,1)S(1)}, bf16[64,2048]{1,0:T(8,128)(2,1)S(1)}, u32[]{:S(2)}, u32[]{:S(2)}) collective-permute-start(bf16[64,2048]{1,0:T(8,128)(2,1)S(1)} %get-tuple-element.40), channel_id=1, source_target_pairs={{0,8},{4,12},{8,0},{12,4},{16,24},{20,28},{24,16},{28,20},{1,9},{5... | collective-permute-start | bytes 786440 | tf_op jit(solution)/shard_map/ppermute | solution.py:18
  126.2 21.8 %collective-permute-start.12 = (bf16[64,2048]{1,0:T(8,128)(2,1)S(1)}, bf16[64,2048]{1,0:T(8,128)(2,1)S(1)}, u32[]{:S(2)}, u32[]{:S(2)}) collective-permute-start(bf16[64,2048]{1,0:T(8,128)(2,1)S(1)} %get-tuple-element.39), channel_id=1, source_target_pairs={{0,12},{4,8},{8,4},{12,0},{16,28},{20,24},{24,20},{28,16},{1,13},{... | collective-permute-start | bytes 786440 | tf_op jit(solution)/shard_map/ppermute | solution.py:18
  128.2 41.7 %collective-permute-start.25 = (f32[128,2]{0,1:T(2,128)S(1)}, f32[128,2]{0,1:T(2,128)S(1)}, u32[]{:S(2)}, u32[]{:S(2)}) collective-permute-start(f32[128,2]{0,1:T(2,128)S(1)} %bitcast.94), channel_id=1, source_target_pairs={{0,16},{4,20},{8,24},{12,28},{16,0},{20,4},{24,8},{28,12},{1,17},{... | collective-permute-start | bytes 3080 | tf_op jit(solution)/shard_map/ppermute | solution.py:18
  132.8 15.2 %copy-start.2 = (bf16[64,2048]{1,0:T(8,128)(2,1)}, bf16[64,2048]{1,0:T(8,128)(2,1)S(1)}, u32[]{:S(2)}) copy-start(bf16[64,2048]{1,0:T(8,128)(2,1)S(1)} %collective-permute-done.10.refs_1_) | copy-start | bytes 786436
  145.4 2.6 %copy-start.4 = (bf16[64,2048]{1,0:T(8,128)(2,1)}, bf16[64,2048]{1,0:T(8,128)(2,1)S(1)}, u32[]{:S(2)}) copy-start(bf16[64,2048]{1,0:T(8,128)(2,1)S(1)} %collective-permute-done.11.refs_2_) | copy-start | bytes 786436
  148.0 0.7 copy-start.7
  163.3 6.6 %copy-start.9 = (bf16[64,2048]{1,0:T(8,128)(2,1)S(1)}, bf16[64,2048]{1,0:T(8,128)(2,1)}, u32[]{:S(2)}) copy-start(bf16[64,2048]{1,0:T(8,128)(2,1)} %get-tuple-element.23) | copy-start | bytes 786436
  163.3 35.9 %collective-permute-start.13 = (bf16[64,2048]{1,0:T(8,128)(2,1)}, bf16[64,2048]{1,0:T(8,128)(2,1)}, u32[]{:S(2)}, u32[]{:S(2)}) collective-permute-start(bf16[64,2048]{1,0:T(8,128)(2,1)} %get-tuple-element.24), channel_id=1, source_target_pairs={{0,4},{4,0},{8,12},{12,8},{16,20},{20,16},{24,28},{28,24},{1,5},{5... | collective-permute-start | bytes 786440 | tf_op jit(solution)/shard_map/ppermute | solution.py:18
  166.5 14.6 %collective-permute-start.19 = (bf16[64,2048]{1,0:T(8,128)(2,1)S(1)}, bf16[64,2048]{1,0:T(8,128)(2,1)S(1)}, u32[]{:S(2)}, u32[]{:S(2)}) collective-permute-start(bf16[64,2048]{1,0:T(8,128)(2,1)S(1)} %get-tuple-element.37), channel_id=1, source_target_pairs={{0,4},{4,0},{8,12},{12,8},{16,20},{20,16},{24,28},{28,24},{1,5},{5... | collective-permute-start | bytes 786440 | tf_op jit(solution)/shard_map/ppermute | solution.py:18
  166.8 14.3 %collective-permute-start.20 = (bf16[64,2048]{1,0:T(8,128)(2,1)S(1)}, bf16[64,2048]{1,0:T(8,128)(2,1)S(1)}, u32[]{:S(2)}, u32[]{:S(2)}) collective-permute-start(bf16[64,2048]{1,0:T(8,128)(2,1)S(1)} %get-tuple-element.36), channel_id=1, source_target_pairs={{0,8},{4,12},{8,0},{12,4},{16,24},{20,28},{24,16},{28,20},{1,9},{5... | collective-permute-start | bytes 786440 | tf_op jit(solution)/shard_map/ppermute | solution.py:18
  166.9 15.8 %collective-permute-start.21 = (bf16[64,2048]{1,0:T(8,128)(2,1)S(1)}, bf16[64,2048]{1,0:T(8,128)(2,1)S(1)}, u32[]{:S(2)}, u32[]{:S(2)}) collective-permute-start(bf16[64,2048]{1,0:T(8,128)(2,1)S(1)} %get-tuple-element.35), channel_id=1, source_target_pairs={{0,12},{4,8},{8,4},{12,0},{16,28},{20,24},{24,20},{28,16},{1,13},{... | collective-permute-start | bytes 786440 | tf_op jit(solution)/shard_map/ppermute | solution.py:18
  170.0 45.1 %collective-permute-start.14 = (bf16[64,2048]{1,0:T(8,128)(2,1)}, bf16[64,2048]{1,0:T(8,128)(2,1)S(1)}, u32[]{:S(2)}, u32[]{:S(2)}) collective-permute-start(bf16[64,2048]{1,0:T(8,128)(2,1)} %get-tuple-element.25), channel_id=1, source_target_pairs={{0,8},{4,12},{8,0},{12,4},{16,24},{20,28},{24,16},{28,20},{1,9},{5... | collective-permute-start | bytes 786440 | tf_op jit(solution)/shard_map/ppermute | solution.py:18
  181.1 1.6 copy-start.3
  181.1 34.0 %collective-permute-start.15 = (bf16[64,2048]{1,0:T(8,128)(2,1)}, bf16[64,2048]{1,0:T(8,128)(2,1)S(1)}, u32[]{:S(2)}, u32[]{:S(2)}) collective-permute-start(bf16[64,2048]{1,0:T(8,128)(2,1)} %get-tuple-element.26), channel_id=1, source_target_pairs={{0,12},{4,8},{8,4},{12,0},{16,28},{20,24},{24,20},{28,16},{1,13},{... | collective-permute-start | bytes 786440 | tf_op jit(solution)/shard_map/ppermute | solution.py:18
  181.1 1.6 copy-start.5
  182.7 0.7 copy-start.6
  198.0 6.6 %collective-permute-start.22 = (bf16[64,2048]{1,0:T(8,128)(2,1)}, bf16[64,2048]{1,0:T(8,128)(2,1)S(1)}, u32[]{:S(2)}, u32[]{:S(2)}) collective-permute-start(bf16[64,2048]{1,0:T(8,128)(2,1)} %get-tuple-element.28), channel_id=1, source_target_pairs={{0,4},{4,0},{8,12},{12,8},{16,20},{20,16},{24,28},{28,24},{1,5},{5... | collective-permute-start | bytes 786440 | tf_op jit(solution)/shard_map/ppermute | solution.py:18
  200.2 9.0 %collective-permute-start.23 = (bf16[64,2048]{1,0:T(8,128)(2,1)}, bf16[64,2048]{1,0:T(8,128)(2,1)S(1)}, u32[]{:S(2)}, u32[]{:S(2)}) collective-permute-start(bf16[64,2048]{1,0:T(8,128)(2,1)} %get-tuple-element.29), channel_id=1, source_target_pairs={{0,8},{4,12},{8,0},{12,4},{16,24},{20,28},{24,16},{28,20},{1,9},{5... | collective-permute-start | bytes 786440 | tf_op jit(solution)/shard_map/ppermute | solution.py:18
  202.6 11.6 %collective-permute-start.24 = (bf16[64,2048]{1,0:T(8,128)(2,1)}, bf16[64,2048]{1,0:T(8,128)(2,1)S(1)}, u32[]{:S(2)}, u32[]{:S(2)}) collective-permute-start(bf16[64,2048]{1,0:T(8,128)(2,1)} %get-tuple-element.30), channel_id=1, source_target_pairs={{0,12},{4,8},{8,4},{12,0},{16,28},{20,24},{24,20},{28,16},{1,13},{... | collective-permute-start | bytes 786440 | tf_op jit(solution)/shard_map/ppermute | solution.py:18
  215.0 15.8 %collective-permute-start.26 = (bf16[128,2048]{1,0:T(8,128)(2,1)S(1)}, bf16[128,2048]{1,0:T(8,128)(2,1)S(1)}, u32[]{:S(2)}, u32[]{:S(2)}) collective-permute-start(bf16[128,2048]{1,0:T(8,128)(2,1)S(1)} %fusion.5), channel_id=1, source_target_pairs={{0,16},{4,20},{8,24},{12,28},{16,0},{20,4},{24,8},{28,12},{1,17},{... | collective-permute-start | bytes 1572872 | tf_op jit(solution)/shard_map/ppermute | solution.py:18

commit v3 on v2

--- a/solution.py
+++ b/solution.py
@@ -110,7 +110,10 @@
 
 def expert_rows(blocks, gate, up, down):
     count = len(blocks)
-    rows, model = blocks[0].shape
+    model = blocks[0].shape[1]
+    heights = [block.shape[0] for block in blocks]
+    starts = [sum(heights[:i]) for i in range(count)]
+    total = sum(heights)
     hidden_width = gate.shape[1]
     tile = 256
     steps = hidden_width // tile
@@ -125,7 +128,7 @@
         @pl.when(step == 0)
         def _():
             for i in range(count):
-                x_all[i * rows : (i + 1) * rows, :] = x_refs[i][...]
+                x_all[starts[i] : starts[i] + heights[i], :] = x_refs[i][...]
 
         x = x_all[...]
         g = jnp.dot(x, g_ref[...], preferred_element_type=F32)
@@ -144,23 +147,23 @@
         @pl.when(step == steps - 1)
         def _():
             for i in range(count):
-                o_refs[i][...] = acc[i * rows : (i + 1) * rows, :].astype(BF16)
-
-    whole = pl.BlockSpec((rows, model), lambda i: (0, 0))
+                o_refs[i][...] = acc[starts[i] : starts[i] + heights[i], :].astype(BF16)
+
+    whole = [pl.BlockSpec((height, model), lambda i: (0, 0)) for height in heights]
     return pl.pallas_call(
         body,
         grid=(steps,),
-        in_specs=[whole] * count
+        in_specs=whole
         + [
             pl.BlockSpec((model, tile), lambda i: (0, i)),
             pl.BlockSpec((model, tile), lambda i: (0, i)),
             pl.BlockSpec((tile, model), lambda i: (i, 0)),
         ],
-        out_specs=[whole] * count,
-        out_shape=[jax.ShapeDtypeStruct((rows, model), BF16)] * count,
+        out_specs=whole,
+        out_shape=[jax.ShapeDtypeStruct((height, model), BF16) for height in heights],
         scratch_shapes=[
-            pltpu.VMEM((count * rows, model), BF16),
-            pltpu.VMEM((count * rows, model), F32),
+            pltpu.VMEM((total, model), BF16),
+            pltpu.VMEM((total, model), F32),
         ],
         name="expert_rows",
     )(*blocks, gate, up, down)
@@ -214,18 +217,23 @@
     chosen_far = swap(chosen, "sp", half)
     slot_far = swap(slot, "sp", half)
     weight_far = swap(weight, "sp", half)
-    place = jnp.arange(half * slots, dtype=jnp.int32)
-    place_expert = me ^ (place // slots)
-    place_slot = place % slots
-
-    def selection(chosen, slot):
+
+    def selection(chosen, slot, first, count):
+        place = jnp.arange(half * count, dtype=jnp.int32)
+        expert = me ^ (place // count)
+        place_slot = first + place % count
         return [
-            (chosen[:, j, None] == place_expert[None]) & (slot[:, j, None] == place_slot[None])
+            (chosen[:, j, None] == expert[None]) & (slot[:, j, None] == place_slot[None])
             for j in range(2)
         ]
 
-    pick = selection(chosen, slot)
-    pick_far = selection(chosen_far, slot_far)
+    block = tokens // 2
+    spans = [slice(b * block, (b + 1) * block) for b in range(2)]
+    pick = selection(chosen, slot, 0, slots)
+    picks_far = [
+        selection(chosen_far[spans[b]], slot_far[spans[b]], b * capacity, capacity)
+        for b in range(2)
+    ]
 
     attended = attend(by_head.reshape(parts * tokens, -1), per, kv_per, width)
     attended, shards = lax.optimization_barrier((attended, shards))
@@ -234,8 +242,6 @@
         whole.append(shards[far])
         for close in range(1, near):
             whole.append(swap(shards[far], "sp", close))
-    own_columns = jnp.concatenate(whole, axis=0)
-    core_columns = swap(own_columns, "dp", 1)
     returned = lax.all_to_all(
         attended.reshape(parts, tokens, per * width), "sp", split_axis=0, concat_axis=0, tiled=True
     )
@@ -245,7 +251,13 @@
     )
 
     chips = columns // 2
-    gathered = jnp.concatenate([rows] + [swap(rows, "dp", 2 * k) for k in range(1, chips)], axis=0)
+    peers = []
+    for k in range(1, chips):
+        peers.append(swap(rows, "dp", 2 * k))
+    _, whole = lax.optimization_barrier((rows, whole))
+    own_columns = jnp.concatenate(whole, axis=0)
+    core_columns = swap(own_columns, "dp", 1)
+    gathered = jnp.concatenate([rows] + peers, axis=0)
     mine = jnp.dot(gathered, own_columns, preferred_element_type=F32).astype(BF16)
     other = jnp.dot(gathered, core_columns, preferred_element_type=F32).astype(BF16)
     first = lax.axis_index("dp") % 2 == 0
@@ -269,23 +281,17 @@
         * norm_gain
     ).astype(BF16)
 
-    normed_far = swap(normed, "sp", half)
-
-    def send(source, picks):
+    crossed = [swap(normed[span], "sp", half) for span in spans]
+
+    def send(source, picks, count):
         chosen_rows = (picks[0] | picks[1]).astype(BF16)
         sent = lax.dot_general(
             chosen_rows, source, (((0,), (0,)), ((), ())), preferred_element_type=F32
         ).astype(BF16)
-        return exchange([sent[k * slots : (k + 1) * slots] for k in range(half)])
+        return exchange([sent[k * count : (k + 1) * count] for k in range(half)])
 
     def exchange(blocks):
-        moved = [blocks[0]]
-        for k in range(1, half):
-            moved.append(swap(blocks[k], "sp", k))
-        return moved
-
-    def serve(blocks):
-        return expert_rows(blocks, expert_gate[0], expert_up[0], expert_down[0])
+        return [blocks[0]] + [swap(blocks[k], "sp", k) for k in range(1, half)]
 
     def combine(results, picks, weight):
         flat = jnp.concatenate(results, axis=0)
@@ -294,14 +300,18 @@
             for j in range(2)
         )
 
-    near_blocks = send(normed, pick)
-    far_blocks = send(normed_far, pick_far)
-    near_results = serve(near_blocks)
-    far_results = serve(far_blocks)
-    near_results = exchange(near_results)
-    far_results = exchange(far_results)
-    crossed = swap(combine(far_results, pick_far, weight_far).astype(BF16), "sp", half)
-    result = mixed_sum + combine(near_results, pick, weight) + crossed.astype(F32)
+    sent = send(normed, pick, slots)
+    for b in range(2):
+        sent = sent + send(crossed[b], picks_far[b], capacity)
+    results = expert_rows(sent, expert_gate[0], expert_up[0], expert_down[0])
+    back = []
+    for b in range(2):
+        far_results = exchange(results[(b + 1) * half : (b + 2) * half])
+        part = combine(far_results, picks_far[b], weight_far[spans[b]]).astype(BF16)
+        back.append(swap(part, "sp", half))
+    near_results = exchange(results[:half])
+    near_part = combine(near_results, pick, weight)
+    result = mixed_sum + near_part + jnp.concatenate(back, axis=0).astype(F32)
     return result.astype(BF16)[None]
 
 

time: 233 us -> 242 us (1.039)
  waiting for transfers between devices: 114 us -> 127 us
  Pallas kernels: 41.9 us -> 33 us
  starting transfers between devices: 50.4 us -> 53.1 us
    all_to_all x1, waiting for transfers between devices: 0.01 us -> 10.5 us  [on_device(): lax.all_to_all(attended.reshape(parts, tokens, per * width), 'sp', split_...]
    pallas_call x2 -> x1, Pallas kernels: 29.2 us -> 20.3 us  [expert_rows(): pl.pallas_call(body, grid=(steps,), in_specs=whole + [pl.BlockSpec((model...]
    ppermute x27 -> x35, starting transfers between devices: 39.5 us -> 42.1 us  [swap(): return lax.ppermute(array, axis, [(i, i ^ bits) for i in range(size)])]
    ppermute x27 -> x35, waiting for transfers between devices: 80.4 us -> 82.3 us  [swap(): return lax.ppermute(array, axis, [(i, i ^ bits) for i in range(size)])]
    unnamed x50 -> x57, local copies, waits for them, and re-layouts: 11.7 us -> 11.8 us
  transfers between devices with their start and end apart: 29 -> 37, of which waited for: 16 -> 20; matrix products, arithmetic and copies ran while one was open for 7% -> 6% of each run, Pallas kernels for 16% -> 3%
where the time goes in v3:
time: 242 us
  waiting for transfers between devices  127 us (52%)
  starting transfers between devices  53.1 us (22%)
  Pallas kernels  33 us (14%)
  local copies, waits for them, and re-layouts  17.5 us (7%)
  matrix products  9.05 us (4%)
    ppermute x35, waiting for transfers between devices, swap(): return lax.ppermute(array, axis, [(i, i ^ bits) for i in range(size)])  82.3 us
    ppermute x35, starting transfers between devices, swap(): return lax.ppermute(array, axis, [(i, i ^ bits) for i in range(size)])  42.1 us
    all_to_all x1, waiting for transfers between devices, on_device(): lax.all_to_all(packed, 'sp', split_axis=0, concat_axis=0, tiled=True)  33.9 us
    pallas_call x1, Pallas kernels, expert_rows(): pl.pallas_call(body, grid=(steps,), in_specs=whole + [pl.BlockSpec((model...  20.3 us
    unnamed x57, local copies, waits for them, and re-layouts  11.8 us
    all_to_all x1, waiting for transfers between devices, on_device(): lax.all_to_all(attended.reshape(parts, tokens, per * width), 'sp', split_...  10.5 us
    pallas_call x1, Pallas kernels, attend(): pl.pallas_call(body, grid=(length // rows,), in_specs=[pl.BlockSpec((rows...  7.84 us
    all_to_all x1, starting transfers between devices, on_device(): lax.all_to_all(packed, 'sp', split_axis=0, concat_axis=0, tiled=True)  7.29 us
  transfers between devices with their start and end apart: 37, of which 20 were waited for; matrix products, arithmetic and copies ran while one was open for 6% of the time, Pallas kernels for 3%

profile of v3, /device:TPU:0, one launch (start us, length us, event | category | flops | bytes accessed | tf_op | source)
XLA Modules:
  0.0 241.6 jit_solution(17103390520250470565)
XLA Ops:
  0.0 2.0 copy.22
  2.0 1.7 copy_bitcast_fusion.1
  3.7 1.0 sine_multiply_fusion
  4.7 4.9 %pack_rows.1 = bf16[8,128,512]{2,1,0:T(8,128)(2,1)} custom-call(bf16[128,2048]{1,0:T(8,128)(2,1)} %bitcast.95, bf16[128,512]{1,0:T(8,128)(2,1)} %get-tuple-element.100.k_ref, bf16[128,512]{1,0:T(8,128)(2,1)} %get-tuple-element.99.v_ref, f32[1,128]{1,0:T(1,128)} %bitcast.103, f32[1,128]{1,0:T(1,128)} %bitcast.104, f32[128,128]{1,0:T(8,128)} %get-tuple-element.80.c_ref, ...), custom_call_target="tpu_custom_call" | custom-call | tf_op jit(solution)/shard_map/pack_rows/pallas_call | solution.py:74
  9.5 7.3 %all-to-all-start = ((bf16[8,128,512]{2,1,0:T(8,128)(2,1)}), bf16[8,128,512]{2,1,0:T(8,128)(2,1)S(1)}, u32[]{:S(2)}, u32[]{:S(2)}) async-start(bf16[8,128,512]{2,1,0:T(8,128)(2,1)} %pack_rows.1), calls=%async_computation | async-start | bytes 2097152 | tf_op jit(solution)/shard_map/all_to_all | solution.py:205
  16.8 2.0 collective-permute-start
  18.9 2.4 collective-permute-start.1
  21.3 33.9 %all-to-all-done = bf16[8,128,512]{2,1,0:T(8,128)(2,1)S(1)} async-done(((bf16[8,128,512]{2,1,0:T(8,128)(2,1)}), bf16[8,128,512]{2,1,0:T(8,128)(2,1)S(1)}, u32[]{:S(2)}, u32[]{:S(2)}) %all-to-all-start) | async-done | bytes 1048608 | tf_op jit(solution)/shard_map/all_to_all | solution.py:205
  55.2 1.0 copy-done
  56.2 7.8 %attend.1 = bf16[1024,256]{1,0:T(8,128)(2,1)} custom-call(bf16[1024,512]{1,0:T(8,128)(2,1)} %bitcast.89, bf16[1024,512]{1,0:T(8,128)(2,1)} %bitcast.90), custom_call_target="tpu_custom_call" | custom-call | tf_op jit(solution)/shard_map/attend/pallas_call | solution.py:98
  64.1 3.7 %all-to-all-start.1 = ((bf16[8,128,256]{2,1,0:T(8,128)(2,1)}), bf16[8,128,256]{2,1,0:T(8,128)(2,1)S(1)}, u32[]{:S(2)}, u32[]{:S(2)}) async-start(bf16[8,128,256]{2,1,0:T(8,128)(2,1)} %bitcast.94), calls=%async_computation.1 | async-start | bytes 1048576 | tf_op jit(solution)/shard_map/all_to_all | solution.py:245
  67.8 2.0 collective-permute-start.4
  69.9 1.9 collective-permute-start.6
  71.9 10.5 %all-to-all-done.1 = bf16[8,128,256]{2,1,0:T(8,128)(2,1)S(1)} async-done(((bf16[8,128,256]{2,1,0:T(8,128)(2,1)}), bf16[8,128,256]{2,1,0:T(8,128)(2,1)S(1)}, u32[]{:S(2)}, u32[]{:S(2)}) %all-to-all-start.1) | async-done | bytes 524320 | tf_op jit(solution)/shard_map/all_to_all | solution.py:245
  82.8 5.6 %collective-permute-done.5 = bf16[256,512]{1,0:T(8,128)(2,1)S(1)} collective-permute-done((bf16[256,512]{1,0:T(8,128)(2,1)S(1)}, bf16[256,512]{1,0:T(8,128)(2,1)S(1)}, u32[]{:S(2)}, u32[]{:S(2)}) %collective-permute-start.5) | collective-permute-done | bytes 262176 | tf_op jit(solution)/shard_map/ppermute | solution.py:18
  88.4 5.6 %collective-permute-done.6 = bf16[256,512]{1,0:T(8,128)(2,1)S(1)} collective-permute-done((bf16[256,512]{1,0:T(8,128)(2,1)S(1)}, bf16[256,512]{1,0:T(8,128)(2,1)S(1)}, u32[]{:S(2)}, u32[]{:S(2)}) %collective-permute-start.6) | collective-permute-done | bytes 262176 | tf_op jit(solution)/shard_map/ppermute | solution.py:18
  94.0 4.4 %collective-permute-done.7 = bf16[256,512]{1,0:T(8,128)(2,1)S(1)} collective-permute-done((bf16[256,512]{1,0:T(8,128)(2,1)S(1)}, bf16[256,512]{1,0:T(8,128)(2,1)S(1)}, u32[]{:S(2)}, u32[]{:S(2)}) %collective-permute-start.7) | collective-permute-done | bytes 262176 | tf_op jit(solution)/shard_map/ppermute | solution.py:18
  105.1 2.4 %collective-permute-start.14 = (s32[128,2]{1,0:T(8,128)S(1)}, s32[128,2]{1,0:T(8,128)S(1)}, u32[]{:S(2)}, u32[]{:S(2)}) collective-permute-start(s32[128,2]{1,0:T(8,128)S(1)} %broadcast_add_fusion), channel_id=1, source_target_pairs={{0,16},{4,20},{8,24},{12,28},{16,0},{20,4},{24,8},{28,12},{1,17},{... | collective-permute-start | bytes 3080 | tf_op jit(solution)/shard_map/ppermute | solution.py:18
  108.1 2.4 collective-permute-start.29
  110.6 1.6 collective-permute-start.3
  112.2 12.0 %collective-permute-done.3 = bf16[128,2048]{1,0:T(8,128)(2,1)S(1)} collective-permute-done((bf16[128,2048]{1,0:T(8,128)(2,1)S(1)}, bf16[128,2048]{1,0:T(8,128)(2,1)S(1)}, u32[]{:S(2)}, u32[]{:S(2)}) %collective-permute-start.3) | collective-permute-done | bytes 524320 | tf_op jit(solution)/shard_map/ppermute | solution.py:18
  124.2 2.3 convolution_convert_fusion.3
  126.5 2.3 broadcast_select_fusion.1
  128.9 1.6 collective-permute-start.9
  130.8 5.2 %collective-permute-done.9 = bf16[128,1024]{1,0:T(8,128)(2,1)S(1)} collective-permute-done((bf16[128,1024]{1,0:T(8,128)(2,1)S(1)}, bf16[128,1024]{1,0:T(8,128)(2,1)S(1)}, u32[]{:S(2)}, u32[]{:S(2)}) %collective-permute-start.9) | collective-permute-done | bytes 262176 | tf_op jit(solution)/shard_map/ppermute | solution.py:18
  139.2 1.5 collective-permute-start.11
  140.7 1.5 collective-permute-start.12
  142.2 7.2 %collective-permute-done.15 = bf16[64,2048]{1,0:T(8,128)(2,1)S(1)} collective-permute-done((bf16[64,2048]{1,0:T(8,128)(2,1)S(1)}, bf16[64,2048]{1,0:T(8,128)(2,1)S(1)}, u32[]{:S(2)}, u32[]{:S(2)}) %collective-permute-start.15) | collective-permute-done | bytes 262176 | tf_op jit(solution)/shard_map/ppermute | solution.py:18
  150.5 12.7 %collective-permute-done.19 = bf16[64,2048]{1,0:T(8,128)(2,1)S(1)} collective-permute-done((bf16[64,2048]{1,0:T(8,128)(2,1)S(1)}, bf16[64,2048]{1,0:T(8,128)(2,1)S(1)}, u32[]{:S(2)}, u32[]{:S(2)}) %collective-permute-start.19) | collective-permute-done | bytes 262176 | tf_op jit(solution)/shard_map/ppermute | solution.py:18
  165.2 2.6 %collective-permute-start.18 = (bf16[32,2048]{1,0:T(8,128)(2,1)S(1)}, bf16[32,2048]{1,0:T(8,128)(2,1)S(1)}, u32[]{:S(2)}, u32[]{:S(2)}) collective-permute-start(bf16[32,2048]{1,0:T(8,128)(2,1)S(1)} %get-tuple-element.73), channel_id=1, source_target_pairs={{0,12},{4,8},{8,4},{12,0},{16,28},{20,24},{24,20},{28,16},{1,13},{... | collective-permute-start | bytes 393224 | tf_op jit(solution)/shard_map/ppermute | solution.py:18
  168.8 2.6 %collective-permute-start.22 = (bf16[32,2048]{1,0:T(8,128)(2,1)S(1)}, bf16[32,2048]{1,0:T(8,128)(2,1)S(1)}, u32[]{:S(2)}, u32[]{:S(2)}) collective-permute-start(bf16[32,2048]{1,0:T(8,128)(2,1)S(1)} %get-tuple-element.67), channel_id=1, source_target_pairs={{0,12},{4,8},{8,4},{12,0},{16,28},{20,24},{24,20},{28,16},{1,13},{... | collective-permute-start | bytes 393224 | tf_op jit(solution)/shard_map/ppermute | solution.py:18
  171.6 3.5 %collective-permute-done.18.refs_7_ = bf16[32,2048]{1,0:T(8,128)(2,1)S(1)} collective-permute-done((bf16[32,2048]{1,0:T(8,128)(2,1)S(1)}, bf16[32,2048]{1,0:T(8,128)(2,1)S(1)}, u32[]{:S(2)}, u32[]{:S(2)}) %collective-permute-start.18) | collective-permute-done | bytes 131104 | tf_op jit(solution)/shard_map/ppermute | solution.py:18
  176.3 1.8 collective-permute-done.22.refs_11_
  178.8 20.3 %expert_rows.1 = (bf16[64,2048]{1,0:T(8,128)(2,1)}, bf16[64,2048]{1,0:T(8,128)(2,1)}, bf16[64,2048]{1,0:T(8,128)(2,1)}, bf16[64,2048]{1,0:T(8,128)(2,1)}, bf16[3...) custom-call(bf16[64,2048]{1,0:T(8,128)(2,1)} %get-tuple-element.64.r, ...), custom_call_target="tpu_custom_call" | custom-call | tf_op jit(solution)/shard_map/expert_rows/pallas_call | solution.py:153
  200.1 1.1 collective-permute-start.26
  201.9 1.7 collective-permute-start.28
  203.6 1.0 collective-permute-start.31
  205.4 1.0 constant_dynamic-update-slice_fusion.11
  207.3 2.1 collective-permute-start.33
  209.4 1.0 collective-permute-start.23
  210.4 1.3 collective-permute-start.24
  212.9 1.9 collective-permute-start.25
  214.7 1.7 collective-permute-start.30
  216.4 7.7 %collective-permute-done.33 = bf16[32,2048]{1,0:T(8,128)(2,1)S(1)} collective-permute-done((bf16[32,2048]{1,0:T(8,128)(2,1)}, bf16[32,2048]{1,0:T(8,128)(2,1)S(1)}, u32[]{:S(2)}, u32[]{:S(2)}) %collective-permute-start.33) | collective-permute-done | bytes 131104 | tf_op jit(solution)/shard_map/ppermute | solution.py:18
  225.5 3.7 %collective-permute-done.24 = bf16[64,2048]{1,0:T(8,128)(2,1)S(1)} collective-permute-done((bf16[64,2048]{1,0:T(8,128)(2,1)}, bf16[64,2048]{1,0:T(8,128)(2,1)S(1)}, u32[]{:S(2)}, u32[]{:S(2)}) %collective-permute-start.24) | collective-permute-done | bytes 262176 | tf_op jit(solution)/shard_map/ppermute | solution.py:18
  229.2 3.8 %collective-permute-done.25 = bf16[64,2048]{1,0:T(8,128)(2,1)S(1)} collective-permute-done((bf16[64,2048]{1,0:T(8,128)(2,1)S(1)}, bf16[64,2048]{1,0:T(8,128)(2,1)S(1)}, u32[]{:S(2)}, u32[]{:S(2)}) %collective-permute-start.25) | collective-permute-done | bytes 262176 | tf_op jit(solution)/shard_map/ppermute | solution.py:18
  233.4 6.8 %collective-permute-done.34 = bf16[64,2048]{1,0:T(8,128)(2,1)S(1)} collective-permute-done((bf16[64,2048]{1,0:T(8,128)(2,1)S(1)}, bf16[64,2048]{1,0:T(8,128)(2,1)S(1)}, u32[]{:S(2)}, u32[]{:S(2)}) %collective-permute-start.34) | collective-permute-done | bytes 262176 | tf_op jit(solution)/shard_map/ppermute | solution.py:18
  240.2 1.4 fusion.4
  (134 shorter events, 23.8 us)
Async XLA Ops:
  3.7 13.1 %copy-start.5 = (bf16[256,512]{1,0:T(8,128)(2,1)S(1)}, bf16[256,512]{1,0:T(8,128)(2,1)}, u32[]{:S(2)}) copy-start(bf16[256,512]{1,0:T(8,128)(2,1)} %param.18) | copy-start | bytes 786436
  9.5 45.7 %all-to-all-start = ((bf16[8,128,512]{2,1,0:T(8,128)(2,1)}), bf16[8,128,512]{2,1,0:T(8,128)(2,1)S(1)}, u32[]{:S(2)}, u32[]{:S(2)}) async-start(bf16[8,128,512]{2,1,0:T(8,128)(2,1)} %pack_rows.1), calls=%async_computation | async-start | bytes 2097152 | tf_op jit(solution)/shard_map/all_to_all | solution.py:205
  16.8 47.2 %collective-permute-start = (bf16[256,512]{1,0:T(8,128)(2,1)S(1)}, bf16[256,512]{1,0:T(8,128)(2,1)S(1)}, u32[]{:S(2)}, u32[]{:S(2)}) collective-permute-start(bf16[256,512]{1,0:T(8,128)(2,1)S(1)} %copy-done.5), channel_id=1, source_target_pairs={{0,8},{4,12},{8,0},{12,4},{16,24},{20,28},{24,16},{28,20},{1,9},{5... | collective-permute-start | bytes 786440 | tf_op jit(solution)/shard_map/ppermute | solution.py:18
  18.9 45.2 %collective-permute-start.1 = (bf16[256,512]{1,0:T(8,128)(2,1)S(1)}, bf16[256,512]{1,0:T(8,128)(2,1)S(1)}, u32[]{:S(2)}, u32[]{:S(2)}) collective-permute-start(bf16[256,512]{1,0:T(8,128)(2,1)S(1)} %copy-done.5), channel_id=1, source_target_pairs={{0,16},{4,20},{8,24},{12,28},{16,0},{20,4},{24,8},{28,12},{1,17},{... | collective-permute-start | bytes 786440 | tf_op jit(solution)/shard_map/ppermute | solution.py:18
  21.2 42.8 %collective-permute-start.2 = (bf16[256,512]{1,0:T(8,128)(2,1)S(1)}, bf16[256,512]{1,0:T(8,128)(2,1)S(1)}, u32[]{:S(2)}, u32[]{:S(2)}) collective-permute-start(bf16[256,512]{1,0:T(8,128)(2,1)S(1)} %copy-done.5), channel_id=1, source_target_pairs={{0,24},{4,28},{8,16},{12,20},{16,8},{20,12},{24,0},{28,4},{1,25},{... | collective-permute-start | bytes 786440 | tf_op jit(solution)/shard_map/ppermute | solution.py:18
  64.1 18.4 %all-to-all-start.1 = ((bf16[8,128,256]{2,1,0:T(8,128)(2,1)}), bf16[8,128,256]{2,1,0:T(8,128)(2,1)S(1)}, u32[]{:S(2)}, u32[]{:S(2)}) async-start(bf16[8,128,256]{2,1,0:T(8,128)(2,1)} %bitcast.94), calls=%async_computation.1 | async-start | bytes 1048576 | tf_op jit(solution)/shard_map/all_to_all | solution.py:245
  67.8 15.0 %collective-permute-start.4 = (bf16[256,512]{1,0:T(8,128)(2,1)S(1)}, bf16[256,512]{1,0:T(8,128)(2,1)S(1)}, u32[]{:S(2)}, u32[]{:S(2)}) collective-permute-start(bf16[256,512]{1,0:T(8,128)(2,1)S(1)} %copy-done.5), channel_id=1, source_target_pairs={{0,4},{4,0},{8,12},{12,8},{16,20},{20,16},{24,28},{28,24},{1,5},{5... | collective-permute-start | bytes 786440 | tf_op jit(solution)/shard_map/ppermute | solution.py:18
  69.8 18.6 %collective-permute-start.5 = (bf16[256,512]{1,0:T(8,128)(2,1)S(1)}, bf16[256,512]{1,0:T(8,128)(2,1)S(1)}, u32[]{:S(2)}, u32[]{:S(2)}) collective-permute-start(bf16[256,512]{1,0:T(8,128)(2,1)S(1)} %collective-permute-done), channel_id=1, source_target_pairs={{0,4},{4,0},{8,12},{12,8},{16,20},{20,16},{24,28},{28,24},{1,5},{5... | collective-permute-start | bytes 786440 | tf_op jit(solution)/shard_map/ppermute | solution.py:18
  69.9 24.1 %collective-permute-start.6 = (bf16[256,512]{1,0:T(8,128)(2,1)S(1)}, bf16[256,512]{1,0:T(8,128)(2,1)S(1)}, u32[]{:S(2)}, u32[]{:S(2)}) collective-permute-start(bf16[256,512]{1,0:T(8,128)(2,1)S(1)} %collective-permute-done.1), channel_id=1, source_target_pairs={{0,4},{4,0},{8,12},{12,8},{16,20},{20,16},{24,28},{28,24},{1,5},{5... | collective-permute-start | bytes 786440 | tf_op jit(solution)/shard_map/ppermute | solution.py:18
  71.8 26.6 %collective-permute-start.7 = (bf16[256,512]{1,0:T(8,128)(2,1)S(1)}, bf16[256,512]{1,0:T(8,128)(2,1)S(1)}, u32[]{:S(2)}, u32[]{:S(2)}) collective-permute-start(bf16[256,512]{1,0:T(8,128)(2,1)S(1)} %collective-permute-done.2), channel_id=1, source_target_pairs={{0,4},{4,0},{8,12},{12,8},{16,20},{20,16},{24,28},{28,24},{1,5},{5... | collective-permute-start | bytes 786440 | tf_op jit(solution)/shard_map/ppermute | solution.py:18
  82.6 21.6 %copy-start.13 = (s32[1,128,2]{1,2,0:T(2,128)S(1)}, s32[1,128,2]{1,2,0:T(2,128)}, u32[]{:S(2)}) copy-start(s32[1,128,2]{1,2,0:T(2,128)} %param.24) | copy-start | bytes 3076
  99.1 9.0 %copy-start.14 = (f32[1,128,2]{1,2,0:T(2,128)S(1)}, f32[1,128,2]{1,2,0:T(2,128)}, u32[]{:S(2)}) copy-start(f32[1,128,2]{1,2,0:T(2,128)} %param.25) | copy-start | bytes 3076
  104.2 20.0 %collective-permute-start.8 = (bf16[2048,512]{1,0:T(8,128)(2,1)}, bf16[2048,512]{1,0:T(8,128)(2,1)}, u32[]{:S(2)}, u32[]{:S(2)}) collective-permute-start(bf16[2048,512]{1,0:T(8,128)(2,1)} %constant_dynamic-update-slice_fusion), channel_id=1, source_target_pairs={{0,1},{1,0},{2,3},{3,2},{4,5},{5,4},{6,7},{7,6},{8,9},{9,8},{10,11... | collective-permute-start | bytes 6291464 | tf_op jit(solution)/shard_map/ppermute | solution.py:18
  105.1 25.4 %collective-permute-start.14 = (s32[128,2]{1,0:T(8,128)S(1)}, s32[128,2]{1,0:T(8,128)S(1)}, u32[]{:S(2)}, u32[]{:S(2)}) collective-permute-start(s32[128,2]{1,0:T(8,128)S(1)} %broadcast_add_fusion), channel_id=1, source_target_pairs={{0,16},{4,20},{8,24},{12,28},{16,0},{20,4},{24,8},{28,12},{1,17},{... | collective-permute-start | bytes 3080 | tf_op jit(solution)/shard_map/ppermute | solution.py:18
  107.5 23.2 %collective-permute-start.13 = (s32[128,2]{0,1:T(2,128)S(1)}, s32[128,2]{0,1:T(2,128)S(1)}, u32[]{:S(2)}, u32[]{:S(2)}) collective-permute-start(s32[128,2]{0,1:T(2,128)S(1)} %bitcast.99), channel_id=1, source_target_pairs={{0,16},{4,20},{8,24},{12,28},{16,0},{20,4},{24,8},{28,12},{1,17},{... | collective-permute-start | bytes 3080 | tf_op jit(solution)/shard_map/ppermute | solution.py:18
  108.1 57.2 %collective-permute-start.29 = (f32[128,2]{0,1:T(2,128)S(1)}, f32[128,2]{0,1:T(2,128)S(1)}, u32[]{:S(2)}, u32[]{:S(2)}) collective-permute-start(f32[128,2]{0,1:T(2,128)S(1)} %bitcast.101), channel_id=1, source_target_pairs={{0,16},{4,20},{8,24},{12,28},{16,0},{20,4},{24,8},{28,12},{1,17},{... | collective-permute-start | bytes 3080 | tf_op jit(solution)/shard_map/ppermute | solution.py:18
  110.6 13.6 %collective-permute-start.3 = (bf16[128,2048]{1,0:T(8,128)(2,1)S(1)}, bf16[128,2048]{1,0:T(8,128)(2,1)S(1)}, u32[]{:S(2)}, u32[]{:S(2)}) collective-permute-start(bf16[128,2048]{1,0:T(8,128)(2,1)S(1)} %bitcast_dynamic-update-slice_fusion), channel_id=1, source_target_pairs={{0,2},{1,3},{2,0},{3,1},{4,6},{5,7},{6,4},{7,5},{8,10},{9,11},{10,... | collective-permute-start | bytes 1572872 | tf_op jit(solution)/shard_map/ppermute | solution.py:18
  128.8 7.3 %copy-start.1 = (bf16[1,128,2048]{2,1,0:T(8,128)(2,1)S(1)}, bf16[1,128,2048]{2,1,0:T(8,128)(2,1)}, u32[]{:S(2)}) copy-start(bf16[1,128,2048]{2,1,0:T(8,128)(2,1)} %param.19) | copy-start | bytes 1572868
  128.8 7.5 %copy-start.12 = (f32[2048]{0:T(1024)S(1)}, f32[2048]{0:T(1024)}, u32[]{:S(2)}) copy-start(f32[2048]{0:T(1024)} %param.20) | copy-start | bytes 24580
  128.9 7.1 %collective-permute-start.9 = (bf16[128,1024]{1,0:T(8,128)(2,1)S(1)}, bf16[128,1024]{1,0:T(8,128)(2,1)S(1)}, u32[]{:S(2)}, u32[]{:S(2)}) collective-permute-start(bf16[128,1024]{1,0:T(8,128)(2,1)S(1)} %pad_maximum_fusion.4), channel_id=1, source_target_pairs={{0,2},{1,3},{2,0},{3,1},{4,6},{5,7},{6,4},{7,5},{8,10},{9,11},{10,... | collective-permute-start | bytes 786440 | tf_op jit(solution)/shard_map/ppermute | solution.py:18
  136.6 12.8 %collective-permute-start.15 = (bf16[64,2048]{1,0:T(8,128)(2,1)S(1)}, bf16[64,2048]{1,0:T(8,128)(2,1)S(1)}, u32[]{:S(2)}, u32[]{:S(2)}) collective-permute-start(bf16[64,2048]{1,0:T(8,128)(2,1)S(1)} %get-tuple-element.72), channel_id=1, source_target_pairs={{0,16},{4,20},{8,24},{12,28},{16,0},{20,4},{24,8},{28,12},{1,17},{... | collective-permute-start | bytes 786440 | tf_op jit(solution)/shard_map/ppermute | solution.py:18
  138.7 26.6 %collective-permute-start.10 = (bf16[64,2048]{1,0:T(8,128)(2,1)S(1)}, bf16[64,2048]{1,0:T(8,128)(2,1)S(1)}, u32[]{:S(2)}, u32[]{:S(2)}) collective-permute-start(bf16[64,2048]{1,0:T(8,128)(2,1)S(1)} %get-tuple-element.63), channel_id=1, source_target_pairs={{0,4},{4,0},{8,12},{12,8},{16,20},{20,16},{24,28},{28,24},{1,5},{5... | collective-permute-start | bytes 786440 | tf_op jit(solution)/shard_map/ppermute | solution.py:18
  139.2 28.7 %collective-permute-start.11 = (bf16[64,2048]{1,0:T(8,128)(2,1)S(1)}, bf16[64,2048]{1,0:T(8,128)(2,1)S(1)}, u32[]{:S(2)}, u32[]{:S(2)}) collective-permute-start(bf16[64,2048]{1,0:T(8,128)(2,1)S(1)} %get-tuple-element.62), channel_id=1, source_target_pairs={{0,8},{4,12},{8,0},{12,4},{16,24},{20,28},{24,16},{28,20},{1,9},{5... | collective-permute-start | bytes 786440 | tf_op jit(solution)/shard_map/ppermute | solution.py:18
  140.7 28.0 %collective-permute-start.12 = (bf16[64,2048]{1,0:T(8,128)(2,1)S(1)}, bf16[64,2048]{1,0:T(8,128)(2,1)S(1)}, u32[]{:S(2)}, u32[]{:S(2)}) collective-permute-start(bf16[64,2048]{1,0:T(8,128)(2,1)S(1)} %get-tuple-element.61), channel_id=1, source_target_pairs={{0,12},{4,8},{8,4},{12,0},{16,28},{20,24},{24,20},{28,16},{1,13},{... | collective-permute-start | bytes 786440 | tf_op jit(solution)/shard_map/ppermute | solution.py:18
  149.4 13.9 %collective-permute-start.19 = (bf16[64,2048]{1,0:T(8,128)(2,1)S(1)}, bf16[64,2048]{1,0:T(8,128)(2,1)S(1)}, u32[]{:S(2)}, u32[]{:S(2)}) collective-permute-start(bf16[64,2048]{1,0:T(8,128)(2,1)S(1)} %get-tuple-element.71), channel_id=1, source_target_pairs={{0,16},{4,20},{8,24},{12,28},{16,0},{20,4},{24,8},{28,12},{1,17},{... | collective-permute-start | bytes 786440 | tf_op jit(solution)/shard_map/ppermute | solution.py:18
  163.3 5.6 %collective-permute-start.16 = (bf16[32,2048]{1,0:T(8,128)(2,1)S(1)}, bf16[32,2048]{1,0:T(8,128)(2,1)S(1)}, u32[]{:S(2)}, u32[]{:S(2)}) collective-permute-start(bf16[32,2048]{1,0:T(8,128)(2,1)S(1)} %get-tuple-element.75), channel_id=1, source_target_pairs={{0,4},{4,0},{8,12},{12,8},{16,20},{20,16},{24,28},{28,24},{1,5},{5... | collective-permute-start | bytes 393224 | tf_op jit(solution)/shard_map/ppermute | solution.py:18
  165.2 6.4 %collective-permute-start.17 = (bf16[32,2048]{1,0:T(8,128)(2,1)S(1)}, bf16[32,2048]{1,0:T(8,128)(2,1)S(1)}, u32[]{:S(2)}, u32[]{:S(2)}) collective-permute-start(bf16[32,2048]{1,0:T(8,128)(2,1)S(1)} %get-tuple-element.74), channel_id=1, source_target_pairs={{0,8},{4,12},{8,0},{12,4},{16,24},{20,28},{24,16},{28,20},{1,9},{5... | collective-permute-start | bytes 393224 | tf_op jit(solution)/shard_map/ppermute | solution.py:18
  165.2 12.9 %copy-start.2 = (bf16[64,2048]{1,0:T(8,128)(2,1)}, bf16[64,2048]{1,0:T(8,128)(2,1)S(1)}, u32[]{:S(2)}) copy-start(bf16[64,2048]{1,0:T(8,128)(2,1)S(1)} %collective-permute-done.10.refs_1_) | copy-start | bytes 786436
  165.2 9.9 %collective-permute-start.18 = (bf16[32,2048]{1,0:T(8,128)(2,1)S(1)}, bf16[32,2048]{1,0:T(8,128)(2,1)S(1)}, u32[]{:S(2)}, u32[]{:S(2)}) collective-permute-start(bf16[32,2048]{1,0:T(8,128)(2,1)S(1)} %get-tuple-element.73), channel_id=1, source_target_pairs={{0,12},{4,8},{8,4},{12,0},{16,28},{20,24},{24,20},{28,16},{1,13},{... | collective-permute-start | bytes 393224 | tf_op jit(solution)/shard_map/ppermute | solution.py:18
  167.9 10.3 %copy-start.3 = (bf16[64,2048]{1,0:T(8,128)(2,1)}, bf16[64,2048]{1,0:T(8,128)(2,1)S(1)}, u32[]{:S(2)}) copy-start(bf16[64,2048]{1,0:T(8,128)(2,1)S(1)} %collective-permute-done.11.refs_2_) | copy-start | bytes 786436
  167.9 7.8 %collective-permute-start.20 = (bf16[32,2048]{1,0:T(8,128)(2,1)S(1)}, bf16[32,2048]{1,0:T(8,128)(2,1)S(1)}, u32[]{:S(2)}, u32[]{:S(2)}) collective-permute-start(bf16[32,2048]{1,0:T(8,128)(2,1)S(1)} %get-tuple-element.69), channel_id=1, source_target_pairs={{0,4},{4,0},{8,12},{12,8},{16,20},{20,16},{24,28},{28,24},{1,5},{5... | collective-permute-start | bytes 393224 | tf_op jit(solution)/shard_map/ppermute | solution.py:18
  168.7 9.4 %copy-start.4 = (bf16[64,2048]{1,0:T(8,128)(2,1)}, bf16[64,2048]{1,0:T(8,128)(2,1)S(1)}, u32[]{:S(2)}) copy-start(bf16[64,2048]{1,0:T(8,128)(2,1)S(1)} %collective-permute-done.12.refs_3_) | copy-start | bytes 786436
  168.7 7.6 %collective-permute-start.21 = (bf16[32,2048]{1,0:T(8,128)(2,1)S(1)}, bf16[32,2048]{1,0:T(8,128)(2,1)S(1)}, u32[]{:S(2)}, u32[]{:S(2)}) collective-permute-start(bf16[32,2048]{1,0:T(8,128)(2,1)S(1)} %get-tuple-element.68), channel_id=1, source_target_pairs={{0,8},{4,12},{8,0},{12,4},{16,24},{20,28},{24,16},{28,20},{1,9},{5... | collective-permute-start | bytes 393224 | tf_op jit(solution)/shard_map/ppermute | solution.py:18
  168.8 9.4 %copy-start.6 = (bf16[32,2048]{1,0:T(8,128)(2,1)}, bf16[32,2048]{1,0:T(8,128)(2,1)S(1)}, u32[]{:S(2)}) copy-start(bf16[32,2048]{1,0:T(8,128)(2,1)S(1)} %collective-permute-done.16.refs_5_) | copy-start | bytes 393220
  168.8 9.3 %collective-permute-start.22 = (bf16[32,2048]{1,0:T(8,128)(2,1)S(1)}, bf16[32,2048]{1,0:T(8,128)(2,1)S(1)}, u32[]{:S(2)}, u32[]{:S(2)}) collective-permute-start(bf16[32,2048]{1,0:T(8,128)(2,1)S(1)} %get-tuple-element.67), channel_id=1, source_target_pairs={{0,12},{4,8},{8,4},{12,0},{16,28},{20,24},{24,20},{28,16},{1,13},{... | collective-permute-start | bytes 393224 | tf_op jit(solution)/shard_map/ppermute | solution.py:18
  171.6 6.6 %copy-start.7 = (bf16[32,2048]{1,0:T(8,128)(2,1)}, bf16[32,2048]{1,0:T(8,128)(2,1)S(1)}, u32[]{:S(2)}) copy-start(bf16[32,2048]{1,0:T(8,128)(2,1)S(1)} %collective-permute-done.17.refs_6_) | copy-start | bytes 393220
  199.1 13.7 %copy-start.15 = (bf16[64,2048]{1,0:T(8,128)(2,1)S(1)}, bf16[64,2048]{1,0:T(8,128)(2,1)}, u32[]{:S(2)}) copy-start(bf16[64,2048]{1,0:T(8,128)(2,1)} %get-tuple-element.46) | copy-start | bytes 786436
  200.1 7.2 %collective-permute-start.26 = (bf16[32,2048]{1,0:T(8,128)(2,1)}, bf16[32,2048]{1,0:T(8,128)(2,1)S(1)}, u32[]{:S(2)}, u32[]{:S(2)}) collective-permute-start(bf16[32,2048]{1,0:T(8,128)(2,1)} %get-tuple-element.48), channel_id=1, source_target_pairs={{0,4},{4,0},{8,12},{12,8},{16,20},{20,16},{24,28},{28,24},{1,5},{5... | collective-permute-start | bytes 393224 | tf_op jit(solution)/shard_map/ppermute | solution.py:18
  201.2 8.2 %collective-permute-start.27 = (bf16[32,2048]{1,0:T(8,128)(2,1)}, bf16[32,2048]{1,0:T(8,128)(2,1)S(1)}, u32[]{:S(2)}, u32[]{:S(2)}) collective-permute-start(bf16[32,2048]{1,0:T(8,128)(2,1)} %get-tuple-element.49), channel_id=1, source_target_pairs={{0,8},{4,12},{8,0},{12,4},{16,24},{20,28},{24,16},{28,20},{1,9},{5... | collective-permute-start | bytes 393224 | tf_op jit(solution)/shard_map/ppermute | solution.py:18
  201.9 8.5 %collective-permute-start.28 = (bf16[32,2048]{1,0:T(8,128)(2,1)}, bf16[32,2048]{1,0:T(8,128)(2,1)S(1)}, u32[]{:S(2)}, u32[]{:S(2)}) collective-permute-start(bf16[32,2048]{1,0:T(8,128)(2,1)} %get-tuple-element.50), channel_id=1, source_target_pairs={{0,12},{4,8},{8,4},{12,0},{16,28},{20,24},{24,20},{28,16},{1,13},{... | collective-permute-start | bytes 393224 | tf_op jit(solution)/shard_map/ppermute | solution.py:18
  203.6 9.2 %collective-permute-start.31 = (bf16[32,2048]{1,0:T(8,128)(2,1)}, bf16[32,2048]{1,0:T(8,128)(2,1)S(1)}, u32[]{:S(2)}, u32[]{:S(2)}) collective-permute-start(bf16[32,2048]{1,0:T(8,128)(2,1)} %get-tuple-element.52), channel_id=1, source_target_pairs={{0,4},{4,0},{8,12},{12,8},{16,20},{20,16},{24,28},{28,24},{1,5},{5... | collective-permute-start | bytes 393224 | tf_op jit(solution)/shard_map/ppermute | solution.py:18
  204.7 10.1 %collective-permute-start.32 = (bf16[32,2048]{1,0:T(8,128)(2,1)}, bf16[32,2048]{1,0:T(8,128)(2,1)S(1)}, u32[]{:S(2)}, u32[]{:S(2)}) collective-permute-start(bf16[32,2048]{1,0:T(8,128)(2,1)} %get-tuple-element.53), channel_id=1, source_target_pairs={{0,8},{4,12},{8,0},{12,4},{16,24},{20,28},{24,16},{28,20},{1,9},{5... | collective-permute-start | bytes 393224 | tf_op jit(solution)/shard_map/ppermute | solution.py:18
  207.3 16.8 %collective-permute-start.33 = (bf16[32,2048]{1,0:T(8,128)(2,1)}, bf16[32,2048]{1,0:T(8,128)(2,1)S(1)}, u32[]{:S(2)}, u32[]{:S(2)}) collective-permute-start(bf16[32,2048]{1,0:T(8,128)(2,1)} %get-tuple-element.54), channel_id=1, source_target_pairs={{0,12},{4,8},{8,4},{12,0},{16,28},{20,24},{24,20},{28,16},{1,13},{... | collective-permute-start | bytes 393224 | tf_op jit(solution)/shard_map/ppermute | solution.py:18
  209.4 16.0 %collective-permute-start.23 = (bf16[64,2048]{1,0:T(8,128)(2,1)}, bf16[64,2048]{1,0:T(8,128)(2,1)S(1)}, u32[]{:S(2)}, u32[]{:S(2)}) collective-permute-start(bf16[64,2048]{1,0:T(8,128)(2,1)} %get-tuple-element.44), channel_id=1, source_target_pairs={{0,4},{4,0},{8,12},{12,8},{16,20},{20,16},{24,28},{28,24},{1,5},{5... | collective-permute-start | bytes 786440 | tf_op jit(solution)/shard_map/ppermute | solution.py:18
  210.4 18.8 %collective-permute-start.24 = (bf16[64,2048]{1,0:T(8,128)(2,1)}, bf16[64,2048]{1,0:T(8,128)(2,1)S(1)}, u32[]{:S(2)}, u32[]{:S(2)}) collective-permute-start(bf16[64,2048]{1,0:T(8,128)(2,1)} %get-tuple-element.45), channel_id=1, source_target_pairs={{0,8},{4,12},{8,0},{12,4},{16,24},{20,28},{24,16},{28,20},{1,9},{5... | collective-permute-start | bytes 786440 | tf_op jit(solution)/shard_map/ppermute | solution.py:18
  212.9 20.1 %collective-permute-start.25 = (bf16[64,2048]{1,0:T(8,128)(2,1)S(1)}, bf16[64,2048]{1,0:T(8,128)(2,1)S(1)}, u32[]{:S(2)}, u32[]{:S(2)}) collective-permute-start(bf16[64,2048]{1,0:T(8,128)(2,1)S(1)} %copy-done.15), channel_id=1, source_target_pairs={{0,12},{4,8},{8,4},{12,0},{16,28},{20,24},{24,20},{28,16},{1,13},{... | collective-permute-start | bytes 786440 | tf_op jit(solution)/shard_map/ppermute | solution.py:18
  214.7 18.6 %collective-permute-start.30 = (bf16[64,2048]{1,0:T(8,128)(2,1)S(1)}, bf16[64,2048]{1,0:T(8,128)(2,1)S(1)}, u32[]{:S(2)}, u32[]{:S(2)}) collective-permute-start(bf16[64,2048]{1,0:T(8,128)(2,1)S(1)} %fusion.7), channel_id=1, source_target_pairs={{0,16},{4,20},{8,24},{12,28},{16,0},{20,4},{24,8},{28,12},{1,17},{... | collective-permute-start | bytes 786440 | tf_op jit(solution)/shard_map/ppermute | solution.py:18
  224.7 15.5 %collective-permute-start.34 = (bf16[64,2048]{1,0:T(8,128)(2,1)S(1)}, bf16[64,2048]{1,0:T(8,128)(2,1)S(1)}, u32[]{:S(2)}, u32[]{:S(2)}) collective-permute-start(bf16[64,2048]{1,0:T(8,128)(2,1)S(1)} %fusion.8), channel_id=1, source_target_pairs={{0,16},{4,20},{8,24},{12,28},{16,0},{20,4},{24,8},{28,12},{1,17},{... | collective-permute-start | bytes 786440 | tf_op jit(solution)/shard_map/ppermute | solution.py:18
  (5 other events, 9.1 us)
